TPU v7x, 256 devices: a 4x2x16 block of a 4x16x16 slice. The times are simulated.
256 devices in a mesh: grp: 2 (over y), ep: 32 (over z, core), tp: 4 (over x).
Axes of the slice: x: 4, y: 2, z: 16, core: 2. Of those that a mesh axis runs over, the one named last changes fastest.
The devices are a block of a 4x16x16 slice.
Arguments:
- mixer_tokens: bfloat16 [32768, 2048], P(('grp', 'ep', 'tp')), parts along dimension 0, may hold values from -6 to 6
- mixer_gain: float32 [2048], replicated, may hold values from 0.1 to 1.9
- proj_in: bfloat16 [2048, 1024], P(None, 'tp'), may hold values from -0.125 to 0.125
- pool_weight: bfloat16 [4, 256, 256], P('tp'), may hold values from -0.375 to 0.375
- pool_scale: float32 [1024], P('tp'), may hold values from 0.1 to 1.9
- proj_out: bfloat16 [1024, 2048], P('tp'), may hold values from -0.1875 to 0.1875
- expert_tokens: bfloat16 [32768, 2048], P(('grp', 'ep', 'tp')), parts along dimension 0, may hold values from -6 to 6
- expert_gain: float32 [2048], replicated, may hold values from 0.1 to 1.9
- expert_route: int32 [32768, 2], P(('grp', 'ep')), parts along dimension 0, may hold values from 0 to 63, as said below
- route_gate: float32 [32768, 2], P(('grp', 'ep')), parts along dimension 0, may hold values from 0.1 to 1
- expert_gate: bfloat16 [64, 2048, 1024], P('ep', None, 'tp'), may hold values from -0.125 to 0.125
- expert_up: bfloat16 [64, 2048, 1024], P('ep', None, 'tp'), may hold values from -0.125 to 0.125
- expert_down: bfloat16 [64, 1024, 2048], P('ep', 'tp'), may hold values from -0.1875 to 0.1875
Outputs:
- mixed_rows: bfloat16 [32768, 2048], P(('grp', 'ep', 'tp')), parts along dimension 0
- moe_rows: bfloat16 [32768, 2048], P(('grp', 'ep', 'tp')), parts along dimension 0
There are 2 independent parts, one for each index of `grp`. A program takes and returns all parts, laid end to end along the dimension named above; an argument that names none is the same for every part. Nothing has to cross between parts.
Inputs may be any that keep to these rules, and one draw needn't show every extreme that they name: `expert_route`: each row names two different experts of one group of 4 consecutive experts. In each aligned block of 128 rows (the routes of the tokens that lie on one device) no expert is named by more than 8 rows, and every expert of a group that the block names at all is named by exactly 8 of its rows; one group, the same in every block, is named in every block, and which other groups a block names varies from block to block.
All inputs are finite; a program needn't handle non-finite values.
Results may differ from a plain program's by a relative error of at most 0.011.
Values may be sent and summed in bfloat16 or wider, within the bound.
No kernel may reach another device: no remote copies, remote signals or barrier semaphores. Data moves between devices by JAX's collectives and lax.ppermute only.
A program may use at most 128 MiB of HBM per device.

v0:
```python
import jax
import jax.numpy as jnp
from jax import lax
from jax.experimental import pallas as pl
from jax.experimental.pallas import tpu as pltpu
from jax.sharding import PartitionSpec as P


GROUP_SIZE = 4

norm_eps = 1e-05
rim_rows = 15
chunks = 2
extra = 128
lift_block = 256
lower_block = 128


def shifted(value, axis, by):
    peers = lax.axis_size(axis)
    pairs = [(i, i + by) for i in range(peers) if 0 <= i + by < peers]
    return lax.ppermute(value, axis, pairs)


def turned(value, axis, by):
    peers = lax.axis_size(axis)
    return lax.ppermute(value, axis, [(i, (i + by) % peers) for i in range(peers)])


def tp_steps():
    peers = lax.axis_size("tp")
    steps = []
    for d in range(1, peers // 2 + 1):
        steps += [d] if 2 * d == peers else [d, -d]
    return steps


def spread(value):
    return [value] + [turned(value, "tp", s) for s in tp_steps()]


def collect(parts):
    arrived = [parts[0]] + [turned(p, "tp", -s) for p, s in zip(parts[1:], tp_steps())]
    total = arrived[0].astype(jnp.float32)
    for part in arrived[1:]:
        total = total + part.astype(jnp.float32)
    return total.astype(jnp.bfloat16)


def layer_norm(values, norm_gain):
    widened = values.astype(jnp.float32)
    center = jnp.mean(widened, axis=-1, keepdims=True)
    spread_of = jnp.mean(jnp.square(widened - center), axis=-1, keepdims=True)
    return ((widened - center) * lax.rsqrt(spread_of + norm_eps) * norm_gain).astype(jnp.bfloat16)


def pooled_diff(extended, windows, first_row):
    widened = extended.astype(jnp.float32)
    row_total = widened.shape[0] - rim_rows
    own_rows = widened[rim_rows:]
    window_sum = own_rows
    for offset in range(1, rim_rows + 1):
        lagged = widened[rim_rows - offset : rim_rows - offset + row_total]
        window_sum = window_sum + jnp.where(offset < windows[None, :], lagged, 0.0)
    position = first_row + jnp.arange(row_total, dtype=jnp.int32)
    covered = jnp.minimum(position[:, None] + 1, windows[None, :]).astype(jnp.float32)
    return (window_sum / covered - own_rows).astype(jnp.bfloat16)


def pool_mix(projected, pool_weight, pool_scale, windows, first_row):
    prior = shifted(projected[-rim_rows:], "ep", 1)
    differences = pooled_diff(jnp.concatenate([prior, projected], axis=0), windows, first_row)
    row_total, local_width = differences.shape
    grouped = differences.reshape(row_total, pool_weight.shape[0], pool_weight.shape[1])
    mixed_groups = jnp.einsum(
        "tgc,gcd->tgd", grouped, pool_weight, preferred_element_type=jnp.float32
    )
    return (mixed_groups.reshape(row_total, local_width) * pool_scale).astype(jnp.bfloat16)


def route_ranks(group, groups):
    rows = group.shape[0]
    named = group[:, None] == jnp.arange(groups, dtype=jnp.int32)
    order = jnp.arange(rows, dtype=jnp.int32)
    before = (order[:, None] > order[None, :]).astype(jnp.bfloat16)
    earlier = jnp.dot(before, named.astype(jnp.bfloat16), preferred_element_type=jnp.float32)
    return jnp.sum(jnp.where(named, earlier, 0.0), axis=1).astype(jnp.int32)


def same_core(value, holders):
    peers = lax.axis_size("ep")
    rings = [list(range(c, peers, holders)) for c in range(holders)]
    return lax.all_to_all(value, "ep", 0, 0, axis_index_groups=rings, tiled=True)


def ring_gather(value):
    half = value.shape[0] // 2
    before = turned(value, "tp", 1)
    after = turned(value, "tp", -1)
    low = turned(before[:half], "tp", 1)
    high = turned(after[half:], "tp", -1)
    return [value, before, after, low, high]


def add_halves(own, lows, highs):
    half = lows[0].shape[0]

    def body(own_ref, *refs):
        out = refs[-1]
        for k, group in enumerate([refs[: len(lows)], refs[len(lows) : -1]]):
            rows = pl.ds(k * half, half)
            total = own_ref[rows].astype(jnp.float32)
            for ref in group:
                total = total + ref[...].astype(jnp.float32)
            out[rows] = total.astype(jnp.bfloat16)

    return pl.pallas_call(
        body, out_shape=jax.ShapeDtypeStruct(own.shape, jnp.bfloat16), name="add_halves"
    )(own, *lows, *highs)


def ring_sum(own, before_low, before_high, after_low, after_high, low, high):
    def joined(x, y):
        return (x.astype(jnp.float32) + y.astype(jnp.float32)).astype(jnp.bfloat16)

    low = turned(low, "tp", 1)
    high = turned(high, "tp", -1)
    after_high = turned(after_high, "tp", 1)
    before_low = turned(before_low, "tp", -1)
    after_low = turned(joined(after_low, low), "tp", 1)
    before_high = turned(joined(before_high, high), "tp", -1)
    return add_halves(own, [after_low, before_low], [after_high, before_high])


def expert_kernel(in_counts, out_counts, holders, local_experts, width, quarter):
    experts = holders * local_experts

    def body(*refs):
        ins, rest = refs[: len(in_counts)], refs[len(in_counts) :]
        weights, rest = rest[: 3 * holders], rest[3 * holders :]
        outs, rest = rest[: len(out_counts)], rest[len(out_counts) :]
        joined, both, downs, hidden, result, in_sem, up_sem, down_sem, out_sem = rest

        def row_copies(refs, counts, make):
            start = 0
            copies = []
            for k, count in enumerate(counts):
                copies.append(make(refs[k], start, count, k))
                start += count
            return copies

        entering = row_copies(
            ins,
            in_counts,
            lambda ref, start, count, k: pltpu.make_async_copy(
                ref, joined.at[pl.ds(start, count)], in_sem.at[k]
            ),
        )
        leaving = row_copies(
            outs,
            out_counts,
            lambda ref, start, count, k: pltpu.make_async_copy(
                result.at[pl.ds(start, count)], ref, out_sem.at[k]
            ),
        )
        lifts, lowers = [], []
        for e in range(experts):
            gate, up, down = weights[3 * (e // local_experts) : 3 * (e // local_experts) + 3]
            i = e % local_experts
            lifts.append(
                pltpu.make_async_copy(gate.at[i], both.at[e, :, pl.ds(0, quarter)], up_sem.at[0, e])
            )
            lifts.append(
                pltpu.make_async_copy(
                    up.at[i], both.at[e, :, pl.ds(quarter, quarter)], up_sem.at[1, e]
                )
            )
            lowers.append(pltpu.make_async_copy(down.at[i], downs.at[e], down_sem.at[e]))
        for copy in lifts[:2] + entering + lifts[2:] + lowers:
            copy.start()
        for copy in entering:
            copy.wait()

        def lift(e, carry):
            for k in range(2):
                part = both.at[e, :, pl.ds(k * quarter, quarter)]
                pltpu.make_async_copy(part, part, up_sem.at[k, e]).wait()

            def lift_rows(i, carry):
                rows = pl.ds(pl.multiple_of(i * lift_block, lift_block), lift_block)
                tail = joined[rows, width:].astype(jnp.float32)
                lane = lax.broadcasted_iota(jnp.int32, tail.shape, 1)
                mine = (lane == e) | (lane == e + GROUP_SIZE)
                weight = jnp.sum(jnp.where(mine, tail, 0.0), axis=1, keepdims=True)
                parts = jnp.dot(
                    joined[rows, :width], both[e], preferred_element_type=jnp.float32
                )
                gate_part = parts[:, :quarter]
                hidden[e, rows] = (
                    gate_part / (1.0 + jnp.exp(-gate_part)) * (parts[:, quarter:] * weight)
                ).astype(jnp.bfloat16)
                return carry

            return lax.fori_loop(0, joined.shape[0] // lift_block, lift_rows, carry)

        lax.fori_loop(0, experts, lift, 0)
        for copy in lowers:
            copy.wait()

        def lower(i, carry):
            rows = pl.ds(pl.multiple_of(i * lower_block, lower_block), lower_block)
            grouped = jnp.concatenate([hidden[e, rows] for e in range(experts)], axis=1)
            total = jnp.dot(
                grouped,
                downs[...].reshape(experts * quarter, width),
                preferred_element_type=jnp.float32,
            )
            result[rows] = total.astype(jnp.bfloat16)
            return carry

        lax.fori_loop(0, joined.shape[0] // lower_block, lower, 0)
        for copy in leaving:
            copy.start()
        for copy in leaving:
            copy.wait()

    return body


def expert_rows(rows, out_counts, sets):
    holders = len(sets)
    local_experts, width, quarter = sets[0][0].shape
    experts = holders * local_experts
    in_counts = [r.shape[0] for r in rows]
    total = sum(in_counts)
    full = rows[0].shape[1]
    anywhere = pl.BlockSpec(memory_space=pl.ANY)
    return pl.pallas_call(
        expert_kernel(in_counts, out_counts, holders, local_experts, width, quarter),
        in_specs=[anywhere] * (len(rows) + 3 * holders),
        out_specs=[anywhere] * len(out_counts),
        out_shape=[jax.ShapeDtypeStruct((count, width), jnp.bfloat16) for count in out_counts],
        scratch_shapes=[
            pltpu.VMEM((total, full), jnp.bfloat16),
            pltpu.VMEM((experts, width, 2 * quarter), jnp.bfloat16),
            pltpu.VMEM((experts, quarter, width), jnp.bfloat16),
            pltpu.VMEM((experts, total, quarter), jnp.bfloat16),
            pltpu.VMEM((total, width), jnp.bfloat16),
            pltpu.SemaphoreType.DMA((len(in_counts),)),
            pltpu.SemaphoreType.DMA((2, experts)),
            pltpu.SemaphoreType.DMA((experts,)),
            pltpu.SemaphoreType.DMA((len(out_counts),)),
        ],
        cost_estimate=pl.CostEstimate(
            flops=6 * total * width * quarter * experts,
            bytes_accessed=6 * width * quarter * experts + 2 * total * (full + width),
            transcendentals=total * quarter * experts,
        ),
        name="experts",
    )(*rows, *[w for one in sets for w in one])


def layer(
    mixer_tokens,
    mixer_gain,
    proj_in,
    pool_weight,
    pool_scale,
    proj_out,
    expert_tokens,
    expert_gain,
    expert_route,
    route_gate,
    expert_gate,
    expert_up,
    expert_down,
):
    ep_count = lax.axis_size("ep")
    tp_index = lax.axis_index("tp")
    ep_index = lax.axis_index("ep")
    own_count, model_width = mixer_tokens.shape
    local_width = proj_in.shape[1]
    group_width = pool_weight.shape[1]
    local_experts = expert_gate.shape[0]
    experts = local_experts * ep_count
    capacity = own_count * GROUP_SIZE // experts
    packet = capacity * GROUP_SIZE // 2
    groups = experts // GROUP_SIZE
    holders = GROUP_SIZE // local_experts
    place = ep_index % holders
    step = packet // chunks

    own_start = tp_index * own_count
    own_route = lax.dynamic_slice_in_dim(expert_route, own_start, own_count, 0)
    own_gates = lax.dynamic_slice_in_dim(route_gate, own_start, own_count, 0)
    group = own_route[:, 0] // GROUP_SIZE
    rank = route_ranks(group, groups)
    slot = rank // step * (groups * step) + group * step + rank % step
    pick = (
        slot[:, None] == jnp.arange(chunks * groups * step, dtype=jnp.int32)
    ).astype(jnp.bfloat16)

    member = (own_route - place * local_experts) % GROUP_SIZE
    lane = jnp.arange(extra, dtype=jnp.int32)
    by_lane = jnp.zeros((own_count, extra), jnp.float32)
    for k in range(2):
        hit = lane[None, :] % GROUP_SIZE == member[:, k : k + 1]
        by_lane = by_lane + jnp.where(hit, own_gates[:, k : k + 1], 0.0)
    high = lax.reduce_precision(by_lane, 8, 7)
    tail = jnp.where(
        lane < GROUP_SIZE, high, jnp.where(lane < 2 * GROUP_SIZE, by_lane - high, 0.0)
    ).astype(jnp.bfloat16)

    normed_expert = layer_norm(expert_tokens, expert_gain)
    extended = jnp.concatenate([normed_expert, tail], axis=1)
    outgoing = []
    for k in range(chunks):
        part = jnp.einsum(
            "ts,td->sd",
            pick[:, k * groups * step : (k + 1) * groups * step],
            extended,
            preferred_element_type=jnp.float32,
        ).astype(jnp.bfloat16)
        outgoing.append(part.reshape(groups, step, model_width + extra))

    outgoing[0], mixer_tokens, expert_gate, expert_up, expert_down = lax.optimization_barrier(
        (outgoing[0], mixer_tokens, expert_gate, expert_up, expert_down)
    )
    own_set = (expert_gate, expert_up, expert_down)
    sets = [own_set]
    for s in range(1, holders):
        pairs = [(i, i - i % holders + (i - s) % holders) for i in range(ep_count)]
        sets.append(tuple(lax.ppermute(w, "ep", pairs) for w in own_set))

    normed_mixer = layer_norm(mixer_tokens, mixer_gain)
    channel = tp_index * local_width + jnp.arange(local_width, dtype=jnp.int32)
    windows = jnp.left_shift(jnp.full_like(channel, 2), channel // group_width)
    gathered = spread(normed_mixer)

    partials = []
    back = []
    for k in range(chunks):
        arrived = same_core(outgoing[k], holders).reshape(-1, model_width + extra)
        rows = ring_gather(arrived)
        count = arrived.shape[0]
        half = count // 2
        partials.append(expert_rows(rows, [count] + [half] * 6, sets))
        summed = ring_sum(*partials[k])
        back.append(same_core(summed.reshape(groups, step, model_width), holders))

    tp_count = lax.axis_size("tp")
    stacked = jnp.stack(gathered)
    blocks = jnp.dot(
        stacked.reshape(-1, model_width), proj_in, preferred_element_type=jnp.float32
    ).astype(jnp.bfloat16)
    blocks = blocks.reshape(tp_count, own_count, local_width)
    source_step = {s % tp_count: r for r, s in enumerate([0] + tp_steps())}
    by_distance = jnp.stack([blocks[source_step[d]] for d in range(tp_count)])
    order = (tp_index - jnp.arange(tp_count, dtype=jnp.int32)) % tp_count
    projected = by_distance[order].reshape(-1, local_width)
    pooled = pool_mix(
        projected, pool_weight, pool_scale, windows, ep_index * projected.shape[0]
    )
    product = jnp.dot(pooled, proj_out, preferred_element_type=jnp.float32).astype(jnp.bfloat16)
    product = product.reshape(tp_count, own_count, model_width)
    parts = [
        lax.dynamic_index_in_dim(product, (tp_index - s) % tp_count, 0, keepdims=False)
        for s in [0] + tp_steps()
    ]
    parts, _ = lax.optimization_barrier((parts, partials[-1][0]))
    mixed_rows = collect(parts)

    total = None
    for k in range(chunks):
        part = jnp.dot(
            pick[:, k * groups * step : (k + 1) * groups * step],
            back[k].reshape(-1, model_width),
            preferred_element_type=jnp.float32,
        )
        total = part if total is None else total + part
    return (mixed_rows, total.astype(jnp.bfloat16))


def solution(mesh):
    return jax.shard_map(
        layer,
        mesh=mesh,
        in_specs=(
            P(("grp", "ep", "tp"), None),
            P(),
            P(None, "tp"),
            P("tp", None, None),
            P("tp"),
            P("tp", None),
            P(("grp", "ep", "tp"), None),
            P(),
            P(("grp", "ep"), None),
            P(("grp", "ep"), None),
            P("ep", None, "tp"),
            P("ep", None, "tp"),
            P("ep", "tp", None),
        ),
        out_specs=(P(("grp", "ep", "tp"), None), P(("grp", "ep", "tp"), None)),
        check_vma=False,
    )
```

profile of v0, /device:TPU:40, one launch (start us, length us, event | category | flops | bytes accessed | tf_op | source)
XLA Modules:
  0.0 262.7 jit_solution(4578047224373098606)
XLA Ops:
  2.5 1.2 convert_reduce_fusion.1
  3.7 1.3 fusion.12
  5.0 1.5 fusion.14
  6.6 1.2 fusion.1
  7.8 24.1 %all-to-all-start = ((bf16[16,8,2176]{2,1,0:T(8,128)(2,1)}), bf16[16,8,2176]{2,1,0:T(8,128)(2,1)S(1)}, u32[]{:S(2)}, u32[]{:S(2)}) async-start(bf16[16,8,2176]{2,1,0:T(8,128)(2,1)} %fusion.1), calls=%async_computation | async-start | bytes 1114112 | tf_op jit(solution)/shard_map/all_to_all | solution.py:93
  32.0 1.2 fusion
  33.9 27.8 %all-to-all-done = bf16[16,8,2176]{2,1,0:T(8,128)(2,1)S(1)} async-done(((bf16[16,8,2176]{2,1,0:T(8,128)(2,1)}), bf16[16,8,2176]{2,1,0:T(8,128)(2,1)S(1)}, u32[]{:S(2)}, u32[]{:S(2)}) %all-to-all-start) | async-done | bytes 557088 | tf_op jit(solution)/shard_map/all_to_all | solution.py:93
  61.7 7.1 %all-to-all-start.1 = ((bf16[16,8,2176]{2,1,0:T(8,128)(2,1)}), bf16[16,8,2176]{2,1,0:T(8,128)(2,1)S(1)}, u32[]{:S(2)}, u32[]{:S(2)}) async-start(bf16[16,8,2176]{2,1,0:T(8,128)(2,1)} %fusion), calls=%async_computation.1 | async-start | bytes 1114112 | tf_op jit(solution)/shard_map/all_to_all | solution.py:93
  69.5 1.7 collective-permute-start.4
  71.3 1.7 collective-permute-start.5
  73.5 1.2 fusion.11
  74.7 10.7 %collective-permute-done.4.refs_1_ = bf16[128,2176]{1,0:T(8,128)(2,1)S(1)} collective-permute-done((bf16[128,2176]{1,0:T(8,128)(2,1)S(1)}, bf16[128,2176]{1,0:T(8,128)(2,1)S(1)}, u32[]{:S(2)}, u32[]{:S(2)}) %collective-permute-start.4) | collective-permute-done | bytes 557088 | tf_op jit(solution)/shard_map/ppermute | solution.py:27
  87.1 2.6 collective-permute-start.7
  91.3 7.2 %all-to-all-done.1 = bf16[16,8,2176]{2,1,0:T(8,128)(2,1)S(1)} async-done(((bf16[16,8,2176]{2,1,0:T(8,128)(2,1)}), bf16[16,8,2176]{2,1,0:T(8,128)(2,1)S(1)}, u32[]{:S(2)}, u32[]{:S(2)}) %all-to-all-start.1) | async-done | bytes 557088 | tf_op jit(solution)/shard_map/all_to_all | solution.py:93
  98.6 1.7 collective-permute-start.14
  100.3 4.3 %collective-permute-done.6.refs_3_ = bf16[64,2176]{1,0:T(8,128)(2,1)} collective-permute-done((bf16[64,2176]{1,0:T(8,128)(2,1)S(1)}, bf16[64,2176]{1,0:T(8,128)(2,1)}, u32[]{:S(2)}, u32[]{:S(2)}) %collective-permute-start.6) | collective-permute-done | bytes 278560 | tf_op jit(solution)/shard_map/ppermute | solution.py:27
  104.6 14.9 %experts.2 = (bf16[128,2048]{1,0:T(8,128)(2,1)}, bf16[64,2048]{1,0:T(8,128)(2,1)}, bf16[64,2048]{1,0:T(8,128)(2,1)}, bf16[64,2048]{1,0:T(8,128)(2,1)}, bf16[64,2...) custom-call(bf16[128,2176]{1,0:T(8,128)(2,1)} %bitcast.85, bf16[128,2176]{1,0:T(8,128)(2,1)} %copy-done.14, ...), custom_call_target="tpu_custom_call" | custom-call | flops 6442450944 | bytes 16908288 | tf_op jit(solution)/shard_map/experts/pallas_call | solution.py:238
  119.8 2.1 collective-permute-start
  122.9 8.5 %collective-permute-done.15.refs_2_ = bf16[128,2176]{1,0:T(8,128)(2,1)} collective-permute-done((bf16[128,2176]{1,0:T(8,128)(2,1)S(1)}, bf16[128,2176]{1,0:T(8,128)(2,1)}, u32[]{:S(2)}, u32[]{:S(2)}) %collective-permute-start.15) | collective-permute-done | bytes 557088 | tf_op jit(solution)/shard_map/ppermute | solution.py:27
  131.4 1.1 collective-permute-start.16
  133.5 1.5 collective-permute-done.28
  136.6 3.0 %collective-permute-start.17 = (bf16[64,2176]{1,0:T(8,128)(2,1)S(1)}, bf16[64,2176]{1,0:T(8,128)(2,1)}, u32[]{:S(2)}, u32[]{:S(2)}) collective-permute-start(bf16[64,2176]{1,0:T(8,128)(2,1)S(1)} %slice.174), channel_id=1, source_target_pairs={{0,3},{1,0},{2,1},{3,2},{4,7},{5,4},{6,5},{7,6},{8,11},{9,8},{10,9... | collective-permute-start | bytes 835592 | tf_op jit(solution)/shard_map/ppermute | solution.py:27
  139.6 5.7 %collective-permute-done.24 = bf16[64,2048]{1,0:T(8,128)(2,1)S(1)} collective-permute-done((bf16[64,2048]{1,0:T(8,128)(2,1)}, bf16[64,2048]{1,0:T(8,128)(2,1)S(1)}, u32[]{:S(2)}, u32[]{:S(2)}) %collective-permute-start.24) | collective-permute-done | bytes 262176 | tf_op jit(solution)/shard_map/ppermute | solution.py:27
  145.3 2.0 collective-permute-start.26
  147.5 3.2 %collective-permute-start.29 = (bf16[64,2048]{1,0:T(8,128)(2,1)S(1)}, bf16[64,2048]{1,0:T(8,128)(2,1)S(1)}, u32[]{:S(2)}, u32[]{:S(2)}) collective-permute-start(bf16[64,2048]{1,0:T(8,128)(2,1)S(1)} %add_convert_fusion.1), channel_id=1, source_target_pairs={{0,3},{1,0},{2,1},{3,2},{4,7},{5,4},{6,5},{7,6},{8,11},{9,8},{10,9... | collective-permute-start | bytes 786440 | tf_op jit(solution)/shard_map/ppermute | solution.py:27
  150.7 3.7 %collective-permute-done.26.refs_1_ = bf16[64,2048]{1,0:T(8,128)(2,1)S(1)} collective-permute-done((bf16[64,2048]{1,0:T(8,128)(2,1)}, bf16[64,2048]{1,0:T(8,128)(2,1)S(1)}, u32[]{:S(2)}, u32[]{:S(2)}) %collective-permute-start.26) | collective-permute-done | bytes 262176 | tf_op jit(solution)/shard_map/ppermute | solution.py:27
  155.1 2.6 pad_maximum_fusion
  157.7 4.3 %collective-permute-done.25.refs_0_ = bf16[64,2048]{1,0:T(8,128)(2,1)S(1)} collective-permute-done((bf16[64,2048]{1,0:T(8,128)(2,1)S(1)}, bf16[64,2048]{1,0:T(8,128)(2,1)S(1)}, u32[]{:S(2)}, u32[]{:S(2)}) %collective-permute-start.25) | collective-permute-done | bytes 262176 | tf_op jit(solution)/shard_map/ppermute | solution.py:27
  162.7 2.3 add_halves.3
  165.0 11.2 %all-to-all-start.3 = ((bf16[16,8,2048]{2,1,0:T(8,128)(2,1)}), bf16[16,8,2048]{2,1,0:T(8,128)(2,1)S(1)}, u32[]{:S(2)}, u32[]{:S(2)}) async-start(bf16[16,8,2048]{2,1,0:T(8,128)(2,1)} %bitcast.76), calls=%async_computation.3 | async-start | bytes 1048576 | tf_op jit(solution)/shard_map/all_to_all | solution.py:93
  176.3 14.9 %experts.3 = (bf16[128,2048]{1,0:T(8,128)(2,1)}, bf16[64,2048]{1,0:T(8,128)(2,1)}, bf16[64,2048]{1,0:T(8,128)(2,1)}, bf16[64,2048]{1,0:T(8,128)(2,1)}, bf16[64,2...) custom-call(bf16[128,2176]{1,0:T(8,128)(2,1)} %bitcast.82, ...), custom_call_target="tpu_custom_call" | custom-call | flops 6442450944 | bytes 16908288 | tf_op jit(solution)/shard_map/experts/pallas_call | solution.py:238
  191.2 1.9 collective-permute-start.22
  193.1 2.6 %convolution_convert_fusion.3 = bf16[512,256]{1,0:T(8,128)(2,1)S(1)} fusion(bf16[512,2048]{1,0:T(8,128)(2,1)} %bitcast.74, bf16[2048,256]{1,0:T(8,128)(2,1)} %param.15), kind=kOutput, calls=%fused_computation.18 | convolution fusion | flops 537001984 | bytes 3407872 | tf_op jit(solution)/shard_map/dot_general | solution.py:353
  196.3 3.0 %collective-permute-start.20 = (bf16[64,2048]{1,0:T(8,128)(2,1)}, bf16[64,2048]{1,0:T(8,128)(2,1)S(1)}, u32[]{:S(2)}, u32[]{:S(2)}) collective-permute-start(bf16[64,2048]{1,0:T(8,128)(2,1)} %get-tuple-element.38), channel_id=1, source_target_pairs={{0,3},{1,0},{2,1},{3,2},{4,7},{5,4},{6,5},{7,6},{8,11},{9,8},{10,9... | collective-permute-start | bytes 786440 | tf_op jit(solution)/shard_map/ppermute | solution.py:27
  199.3 1.4 collective-permute-done.22
  200.8 3.1 %collective-permute-start.23 = (bf16[64,2048]{1,0:T(8,128)(2,1)S(1)}, bf16[64,2048]{1,0:T(8,128)(2,1)}, u32[]{:S(2)}, u32[]{:S(2)}) collective-permute-start(bf16[64,2048]{1,0:T(8,128)(2,1)S(1)} %add_convert_fusion.3), channel_id=1, source_target_pairs={{0,3},{1,0},{2,1},{3,2},{4,7},{5,4},{6,5},{7,6},{8,11},{9,8},{10,9... | collective-permute-start | bytes 786440 | tf_op jit(solution)/shard_map/ppermute | solution.py:27
  203.8 2.4 collective-permute-done.18
  207.1 1.3 collective-permute-start.3
  209.3 4.7 %collective-permute-done.19.refs_0_ = bf16[64,2048]{1,0:T(8,128)(2,1)S(1)} collective-permute-done((bf16[64,2048]{1,0:T(8,128)(2,1)S(1)}, bf16[64,2048]{1,0:T(8,128)(2,1)S(1)}, u32[]{:S(2)}, u32[]{:S(2)}) %collective-permute-start.19) | collective-permute-done | bytes 262176 | tf_op jit(solution)/shard_map/ppermute | solution.py:27
  214.7 2.3 add_halves.2
  217.1 11.5 %all-to-all-start.2 = ((bf16[16,8,2048]{2,1,0:T(8,128)(2,1)}), bf16[16,8,2048]{2,1,0:T(8,128)(2,1)S(1)}, u32[]{:S(2)}, u32[]{:S(2)}) async-start(bf16[16,8,2048]{2,1,0:T(8,128)(2,1)} %bitcast.77), calls=%async_computation.2 | async-start | bytes 1048576 | tf_op jit(solution)/shard_map/all_to_all | solution.py:93
  228.6 4.2 %convolution_convert_fusion.2 = bf16[512,2048]{1,0:T(8,128)(2,1)} fusion(bf16[256,2048]{1,0:T(8,128)(2,1)S(1)} %copy-done, f32[256]{0:T(256)S(1)} %copy-done.19, f32[527,256]{1,0:T(8,128)S(1)} %maximum_convert_fusion, s32[256]{0:T(256)S(1)} %fusion.79, s32[512]{0:T(512)S(1)} %add_add_fusion, pred[256]{0:T(512)(128)(4,1)S(1)} %get-tuple-element.62, ...), kind=kOutput, calls=%fused_computation.5 | convolution fusion | flops 609878016 | bytes 11677184 | tf_op jit(solution)/shard_map/dot_general | solution.py:364
  232.8 1.7 dynamic-slice_bitcast_fusion
  234.5 2.8 %collective-permute-start.11 = (bf16[128,2048]{1,0:T(8,128)(2,1)S(1)}, bf16[128,2048]{1,0:T(8,128)(2,1)S(1)}, u32[]{:S(2)}, u32[]{:S(2)}) collective-permute-start(bf16[128,2048]{1,0:T(8,128)(2,1)S(1)} %get-tuple-element.31), channel_id=1, source_target_pairs={{0,3},{1,0},{2,1},{3,2},{4,7},{5,4},{6,5},{7,6},{8,11},{9,8},{10,9... | collective-permute-start | bytes 1572872 | tf_op jit(solution)/shard_map/ppermute | solution.py:27
  237.3 1.6 collective-permute-start.13
  238.9 17.9 %collective-permute-done.11 = bf16[128,2048]{1,0:T(8,128)(2,1)S(1)} collective-permute-done((bf16[128,2048]{1,0:T(8,128)(2,1)S(1)}, bf16[128,2048]{1,0:T(8,128)(2,1)S(1)}, u32[]{:S(2)}, u32[]{:S(2)}) %collective-permute-start.11) | collective-permute-done | bytes 524320 | tf_op jit(solution)/shard_map/ppermute | solution.py:27
  256.7 3.4 %collective-permute-done.12 = bf16[128,2048]{1,0:T(8,128)(2,1)S(1)} collective-permute-done((bf16[128,2048]{1,0:T(8,128)(2,1)S(1)}, bf16[128,2048]{1,0:T(8,128)(2,1)S(1)}, u32[]{:S(2)}, u32[]{:S(2)}) %collective-permute-start.12) | collective-permute-done | bytes 524320 | tf_op jit(solution)/shard_map/ppermute | solution.py:27
  260.2 1.1 add_convert_fusion
  (124 shorter events, 17.0 us)
Async XLA Ops:
  0.6 227.9 %copy-start = (bf16[256,2048]{1,0:T(8,128)(2,1)S(1)}, bf16[256,2048]{1,0:T(8,128)(2,1)}, u32[]{:S(2)}) copy-start(bf16[256,2048]{1,0:T(8,128)(2,1)} %param.18) | copy-start | bytes 3145732
  5.0 28.7 %copy-start.1 = (bf16[128,2048]{1,0:T(8,128)(2,1)S(1)}, bf16[128,2048]{1,0:T(8,128)(2,1)}, u32[]{:S(2)}) copy-start(bf16[128,2048]{1,0:T(8,128)(2,1)} %param.13) | copy-start | bytes 1572868
  7.8 61.3 %copy-start.16 = (f32[2048]{0:T(1024)S(1)}, f32[2048]{0:T(1024)}, u32[]{:S(2)}) copy-start(f32[2048]{0:T(1024)} %param.14) | copy-start | bytes 24580
  7.8 53.8 %all-to-all-start = ((bf16[16,8,2176]{2,1,0:T(8,128)(2,1)}), bf16[16,8,2176]{2,1,0:T(8,128)(2,1)S(1)}, u32[]{:S(2)}, u32[]{:S(2)}) async-start(bf16[16,8,2176]{2,1,0:T(8,128)(2,1)} %fusion.1), calls=%async_computation | async-start | bytes 1114112 | tf_op jit(solution)/shard_map/all_to_all | solution.py:93
  33.1 56.6 %collective-permute-start.10 = (bf16[2,256,2048]{2,1,0:T(8,128)(2,1)}, bf16[2,256,2048]{2,1,0:T(8,128)(2,1)}, u32[]{:S(2)}, u32[]{:S(2)}) collective-permute-start(bf16[2,256,2048]{2,1,0:T(8,128)(2,1)} %refs_7_.1), channel_id=1, source_target_pairs={{0,4},{4,0},{8,12},{12,8},{16,20},{20,16},{24,28},{28,24},{32,36},... | collective-permute-start | bytes 6291464 | tf_op jit(solution)/shard_map/ppermute | solution.py:333
  33.1 57.2 %collective-permute-start.8 = (bf16[2,2048,256]{2,1,0:T(8,128)(2,1)}, bf16[2,2048,256]{2,1,0:T(8,128)(2,1)}, u32[]{:S(2)}, u32[]{:S(2)}) collective-permute-start(bf16[2,2048,256]{2,1,0:T(8,128)(2,1)} %refs_5_.1), channel_id=1, source_target_pairs={{0,4},{4,0},{8,12},{12,8},{16,20},{20,16},{24,28},{28,24},{32,36},... | collective-permute-start | bytes 6291464 | tf_op jit(solution)/shard_map/ppermute | solution.py:333
  33.6 65.0 %collective-permute-start.9 = (bf16[2,2048,256]{2,1,0:T(8,128)(2,1)}, bf16[2,2048,256]{2,1,0:T(8,128)(2,1)}, u32[]{:S(2)}, u32[]{:S(2)}) collective-permute-start(bf16[2,2048,256]{2,1,0:T(8,128)(2,1)} %refs_6_.1), channel_id=1, source_target_pairs={{0,4},{4,0},{8,12},{12,8},{16,20},{20,16},{24,28},{28,24},{32,36},... | collective-permute-start | bytes 6291464 | tf_op jit(solution)/shard_map/ppermute | solution.py:333
  61.7 23.7 %copy-start.3 = (bf16[16,8,2176]{2,1,0:T(8,128)(2,1)}, bf16[16,8,2176]{2,1,0:T(8,128)(2,1)S(1)}, u32[]{:S(2)}) copy-start(bf16[16,8,2176]{2,1,0:T(8,128)(2,1)S(1)} %all-to-all-done) | copy-start | bytes 1671172
  61.7 36.9 %all-to-all-start.1 = ((bf16[16,8,2176]{2,1,0:T(8,128)(2,1)}), bf16[16,8,2176]{2,1,0:T(8,128)(2,1)S(1)}, u32[]{:S(2)}, u32[]{:S(2)}) async-start(bf16[16,8,2176]{2,1,0:T(8,128)(2,1)} %fusion), calls=%async_computation.1 | async-start | bytes 1114112 | tf_op jit(solution)/shard_map/all_to_all | solution.py:93
  69.5 15.8 %collective-permute-start.4 = (bf16[128,2176]{1,0:T(8,128)(2,1)S(1)}, bf16[128,2176]{1,0:T(8,128)(2,1)S(1)}, u32[]{:S(2)}, u32[]{:S(2)}) collective-permute-start(bf16[128,2176]{1,0:T(8,128)(2,1)S(1)} %bitcast.83), channel_id=1, source_target_pairs={{0,1},{1,2},{2,3},{3,0},{4,5},{5,6},{6,7},{7,4},{8,9},{9,10},{10,1... | collective-permute-start | bytes 1671176 | tf_op jit(solution)/shard_map/ppermute | solution.py:27
  71.3 14.4 %collective-permute-start.5 = (bf16[128,2176]{1,0:T(8,128)(2,1)S(1)}, bf16[128,2176]{1,0:T(8,128)(2,1)S(1)}, u32[]{:S(2)}, u32[]{:S(2)}) collective-permute-start(bf16[128,2176]{1,0:T(8,128)(2,1)S(1)} %bitcast.84), channel_id=1, source_target_pairs={{0,3},{1,0},{2,1},{3,2},{4,7},{5,4},{6,5},{7,6},{8,11},{9,8},{10,9... | collective-permute-start | bytes 1671176 | tf_op jit(solution)/shard_map/ppermute | solution.py:27
  85.4 19.3 %collective-permute-start.6 = (bf16[64,2176]{1,0:T(8,128)(2,1)S(1)}, bf16[64,2176]{1,0:T(8,128)(2,1)}, u32[]{:S(2)}, u32[]{:S(2)}) collective-permute-start(bf16[64,2176]{1,0:T(8,128)(2,1)S(1)} %slice.171), channel_id=1, source_target_pairs={{0,1},{1,2},{2,3},{3,0},{4,5},{5,6},{6,7},{7,4},{8,9},{9,10},{10,1... | collective-permute-start | bytes 835592 | tf_op jit(solution)/shard_map/ppermute | solution.py:27
  87.1 17.5 %collective-permute-start.7 = (bf16[64,2176]{1,0:T(8,128)(2,1)}, bf16[64,2176]{1,0:T(8,128)(2,1)}, u32[]{:S(2)}, u32[]{:S(2)}) collective-permute-start(bf16[64,2176]{1,0:T(8,128)(2,1)} %slice.172), channel_id=1, source_target_pairs={{0,3},{1,0},{2,1},{3,2},{4,7},{5,4},{6,5},{7,6},{8,11},{9,8},{10,9... | collective-permute-start | bytes 835592 | tf_op jit(solution)/shard_map/ppermute | solution.py:27
  89.7 46.9 %collective-permute-start.1 = (bf16[128,2048]{1,0:T(8,128)(2,1)}, bf16[128,2048]{1,0:T(8,128)(2,1)S(1)}, u32[]{:S(2)}, u32[]{:S(2)}) collective-permute-start(bf16[128,2048]{1,0:T(8,128)(2,1)} %fusion.11), channel_id=1, source_target_pairs={{0,3},{1,0},{2,1},{3,2},{4,7},{5,4},{6,5},{7,6},{8,11},{9,8},{10,9... | collective-permute-start | bytes 1572872 | tf_op jit(solution)/shard_map/ppermute | solution.py:27
  90.4 57.0 %collective-permute-start.2 = (bf16[128,2048]{1,0:T(8,128)(2,1)}, bf16[128,2048]{1,0:T(8,128)(2,1)}, u32[]{:S(2)}, u32[]{:S(2)}) collective-permute-start(bf16[128,2048]{1,0:T(8,128)(2,1)} %fusion.11), channel_id=1, source_target_pairs={{0,2},{1,3},{2,0},{3,1},{4,6},{5,7},{6,4},{7,5},{8,10},{9,11},{10,... | collective-permute-start | bytes 1572872 | tf_op jit(solution)/shard_map/ppermute | solution.py:27
  98.6 20.9 %copy-start.2 = (bf16[16,8,2176]{2,1,0:T(8,128)(2,1)}, bf16[16,8,2176]{2,1,0:T(8,128)(2,1)S(1)}, u32[]{:S(2)}) copy-start(bf16[16,8,2176]{2,1,0:T(8,128)(2,1)S(1)} %all-to-all-done.1) | copy-start | bytes 1671172
  98.6 21.2 %copy-start.4 = (bf16[128,2048]{1,0:T(8,128)(2,1)S(1)}, bf16[128,2048]{1,0:T(8,128)(2,1)}, u32[]{:S(2)}) copy-start(bf16[128,2048]{1,0:T(8,128)(2,1)} %fusion.11) | copy-start | bytes 1572868
  98.6 21.1 %collective-permute-start.14 = (bf16[128,2176]{1,0:T(8,128)(2,1)S(1)}, bf16[128,2176]{1,0:T(8,128)(2,1)}, u32[]{:S(2)}, u32[]{:S(2)}) collective-permute-start(bf16[128,2176]{1,0:T(8,128)(2,1)S(1)} %bitcast.80), channel_id=1, source_target_pairs={{0,1},{1,2},{2,3},{3,0},{4,5},{5,6},{6,7},{7,4},{8,9},{9,10},{10,1... | collective-permute-start | bytes 1671176 | tf_op jit(solution)/shard_map/ppermute | solution.py:27
  104.6 26.8 %collective-permute-start.15 = (bf16[128,2176]{1,0:T(8,128)(2,1)S(1)}, bf16[128,2176]{1,0:T(8,128)(2,1)}, u32[]{:S(2)}, u32[]{:S(2)}) collective-permute-start(bf16[128,2176]{1,0:T(8,128)(2,1)S(1)} %bitcast.81), channel_id=1, source_target_pairs={{0,3},{1,0},{2,1},{3,2},{4,7},{5,4},{6,5},{7,6},{8,11},{9,8},{10,9... | collective-permute-start | bytes 1671176 | tf_op jit(solution)/shard_map/ppermute | solution.py:27
  119.5 27.8 %copy-start.5 = (bf16[64,2048]{1,0:T(8,128)(2,1)S(1)}, bf16[64,2048]{1,0:T(8,128)(2,1)}, u32[]{:S(2)}) copy-start(bf16[64,2048]{1,0:T(8,128)(2,1)} %get-tuple-element.42) | copy-start | bytes 786436
  119.5 27.8 %copy-start.17 = (bf16[64,2048]{1,0:T(8,128)(2,1)S(1)}, bf16[64,2048]{1,0:T(8,128)(2,1)}, u32[]{:S(2)}) copy-start(bf16[64,2048]{1,0:T(8,128)(2,1)} %get-tuple-element.45) | copy-start | bytes 786436
  119.6 15.4 %collective-permute-start.28 = (bf16[64,2048]{1,0:T(8,128)(2,1)}, bf16[64,2048]{1,0:T(8,128)(2,1)S(1)}, u32[]{:S(2)}, u32[]{:S(2)}) collective-permute-start(bf16[64,2048]{1,0:T(8,128)(2,1)} %get-tuple-element.47), channel_id=1, source_target_pairs={{0,3},{1,0},{2,1},{3,2},{4,7},{5,4},{6,5},{7,6},{8,11},{9,8},{10,9... | collective-permute-start | bytes 786440 | tf_op jit(solution)/shard_map/ppermute | solution.py:27
  119.8 27.8 %collective-permute-start = (bf16[128,2048]{1,0:T(8,128)(2,1)S(1)}, bf16[128,2048]{1,0:T(8,128)(2,1)S(1)}, u32[]{:S(2)}, u32[]{:S(2)}) collective-permute-start(bf16[128,2048]{1,0:T(8,128)(2,1)S(1)} %copy-done.4), channel_id=1, source_target_pairs={{0,1},{1,2},{2,3},{3,0},{4,5},{5,6},{6,7},{7,4},{8,9},{9,10},{10,1... | collective-permute-start | bytes 1572872 | tf_op jit(solution)/shard_map/ppermute | solution.py:27
  131.4 44.9 %collective-permute-start.16 = (bf16[64,2176]{1,0:T(8,128)(2,1)S(1)}, bf16[64,2176]{1,0:T(8,128)(2,1)}, u32[]{:S(2)}, u32[]{:S(2)}) collective-permute-start(bf16[64,2176]{1,0:T(8,128)(2,1)S(1)} %slice.173), channel_id=1, source_target_pairs={{0,1},{1,2},{2,3},{3,0},{4,5},{5,6},{6,7},{7,4},{8,9},{9,10},{10,1... | collective-permute-start | bytes 835592 | tf_op jit(solution)/shard_map/ppermute | solution.py:27
  135.0 10.3 %collective-permute-start.24 = (bf16[64,2048]{1,0:T(8,128)(2,1)}, bf16[64,2048]{1,0:T(8,128)(2,1)S(1)}, u32[]{:S(2)}, u32[]{:S(2)}) collective-permute-start(bf16[64,2048]{1,0:T(8,128)(2,1)} %get-tuple-element.43), channel_id=1, source_target_pairs={{0,1},{1,2},{2,3},{3,0},{4,5},{5,6},{6,7},{7,4},{8,9},{9,10},{10,1... | collective-permute-start | bytes 786440 | tf_op jit(solution)/shard_map/ppermute | solution.py:27
  136.6 39.6 %collective-permute-start.17 = (bf16[64,2176]{1,0:T(8,128)(2,1)S(1)}, bf16[64,2176]{1,0:T(8,128)(2,1)}, u32[]{:S(2)}, u32[]{:S(2)}) collective-permute-start(bf16[64,2176]{1,0:T(8,128)(2,1)S(1)} %slice.174), channel_id=1, source_target_pairs={{0,3},{1,0},{2,1},{3,2},{4,7},{5,4},{6,5},{7,6},{8,11},{9,8},{10,9... | collective-permute-start | bytes 835592 | tf_op jit(solution)/shard_map/ppermute | solution.py:27
  145.3 9.1 %collective-permute-start.26 = (bf16[64,2048]{1,0:T(8,128)(2,1)}, bf16[64,2048]{1,0:T(8,128)(2,1)S(1)}, u32[]{:S(2)}, u32[]{:S(2)}) collective-permute-start(bf16[64,2048]{1,0:T(8,128)(2,1)} %get-tuple-element.44), channel_id=1, source_target_pairs={{0,3},{1,0},{2,1},{3,2},{4,7},{5,4},{6,5},{7,6},{8,11},{9,8},{10,9... | collective-permute-start | bytes 786440 | tf_op jit(solution)/shard_map/ppermute | solution.py:27
  147.4 10.3 %collective-permute-start.27 = (bf16[64,2048]{1,0:T(8,128)(2,1)S(1)}, bf16[64,2048]{1,0:T(8,128)(2,1)S(1)}, u32[]{:S(2)}, u32[]{:S(2)}) collective-permute-start(bf16[64,2048]{1,0:T(8,128)(2,1)S(1)} %copy-done.17), channel_id=1, source_target_pairs={{0,1},{1,2},{2,3},{3,0},{4,5},{5,6},{6,7},{7,4},{8,9},{9,10},{10,1... | collective-permute-start | bytes 786440 | tf_op jit(solution)/shard_map/ppermute | solution.py:27
  147.5 10.2 %collective-permute-start.29 = (bf16[64,2048]{1,0:T(8,128)(2,1)S(1)}, bf16[64,2048]{1,0:T(8,128)(2,1)S(1)}, u32[]{:S(2)}, u32[]{:S(2)}) collective-permute-start(bf16[64,2048]{1,0:T(8,128)(2,1)S(1)} %add_convert_fusion.1), channel_id=1, source_target_pairs={{0,3},{1,0},{2,1},{3,2},{4,7},{5,4},{6,5},{7,6},{8,11},{9,8},{10,9... | collective-permute-start | bytes 786440 | tf_op jit(solution)/shard_map/ppermute | solution.py:27
  154.4 7.6 %collective-permute-start.25 = (bf16[64,2048]{1,0:T(8,128)(2,1)S(1)}, bf16[64,2048]{1,0:T(8,128)(2,1)S(1)}, u32[]{:S(2)}, u32[]{:S(2)}) collective-permute-start(bf16[64,2048]{1,0:T(8,128)(2,1)S(1)} %add_convert_fusion.2), channel_id=1, source_target_pairs={{0,1},{1,2},{2,3},{3,0},{4,5},{5,6},{6,7},{7,4},{8,9},{9,10},{10,1... | collective-permute-start | bytes 786440 | tf_op jit(solution)/shard_map/ppermute | solution.py:27
  165.0 52.0 %all-to-all-start.3 = ((bf16[16,8,2048]{2,1,0:T(8,128)(2,1)}), bf16[16,8,2048]{2,1,0:T(8,128)(2,1)S(1)}, u32[]{:S(2)}, u32[]{:S(2)}) async-start(bf16[16,8,2048]{2,1,0:T(8,128)(2,1)} %bitcast.76), calls=%async_computation.3 | async-start | bytes 1048576 | tf_op jit(solution)/shard_map/all_to_all | solution.py:93
  191.2 9.5 %collective-permute-start.22 = (bf16[64,2048]{1,0:T(8,128)(2,1)}, bf16[64,2048]{1,0:T(8,128)(2,1)S(1)}, u32[]{:S(2)}, u32[]{:S(2)}) collective-permute-start(bf16[64,2048]{1,0:T(8,128)(2,1)} %get-tuple-element.41), channel_id=1, source_target_pairs={{0,3},{1,0},{2,1},{3,2},{4,7},{5,4},{6,5},{7,6},{8,11},{9,8},{10,9... | collective-permute-start | bytes 786440 | tf_op jit(solution)/shard_map/ppermute | solution.py:27
  193.1 7.6 %copy-start.7 = (bf16[64,2048]{1,0:T(8,128)(2,1)S(1)}, bf16[64,2048]{1,0:T(8,128)(2,1)}, u32[]{:S(2)}) copy-start(bf16[64,2048]{1,0:T(8,128)(2,1)} %get-tuple-element.40) | copy-start | bytes 786436
  193.1 13.2 %copy-start.6 = (bf16[64,2048]{1,0:T(8,128)(2,1)S(1)}, bf16[64,2048]{1,0:T(8,128)(2,1)}, u32[]{:S(2)}) copy-start(bf16[64,2048]{1,0:T(8,128)(2,1)} %get-tuple-element.36) | copy-start | bytes 786436
  195.7 10.5 %collective-permute-start.18 = (bf16[64,2048]{1,0:T(8,128)(2,1)S(1)}, bf16[64,2048]{1,0:T(8,128)(2,1)S(1)}, u32[]{:S(2)}, u32[]{:S(2)}) collective-permute-start(bf16[64,2048]{1,0:T(8,128)(2,1)S(1)} %copy-done.18), channel_id=1, source_target_pairs={{0,1},{1,2},{2,3},{3,0},{4,5},{5,6},{6,7},{7,4},{8,9},{9,10},{10,1... | collective-permute-start | bytes 786440 | tf_op jit(solution)/shard_map/ppermute | solution.py:27
  196.3 13.0 %collective-permute-start.20 = (bf16[64,2048]{1,0:T(8,128)(2,1)}, bf16[64,2048]{1,0:T(8,128)(2,1)S(1)}, u32[]{:S(2)}, u32[]{:S(2)}) collective-permute-start(bf16[64,2048]{1,0:T(8,128)(2,1)} %get-tuple-element.38), channel_id=1, source_target_pairs={{0,3},{1,0},{2,1},{3,2},{4,7},{5,4},{6,5},{7,6},{8,11},{9,8},{10,9... | collective-permute-start | bytes 786440 | tf_op jit(solution)/shard_map/ppermute | solution.py:27
  199.3 10.0 %collective-permute-start.21 = (bf16[64,2048]{1,0:T(8,128)(2,1)}, bf16[64,2048]{1,0:T(8,128)(2,1)}, u32[]{:S(2)}, u32[]{:S(2)}) collective-permute-start(bf16[64,2048]{1,0:T(8,128)(2,1)} %get-tuple-element.39), channel_id=1, source_target_pairs={{0,1},{1,2},{2,3},{3,0},{4,5},{5,6},{6,7},{7,4},{8,9},{9,10},{10,1... | collective-permute-start | bytes 786440 | tf_op jit(solution)/shard_map/ppermute | solution.py:27
  200.8 8.6 %collective-permute-start.23 = (bf16[64,2048]{1,0:T(8,128)(2,1)S(1)}, bf16[64,2048]{1,0:T(8,128)(2,1)}, u32[]{:S(2)}, u32[]{:S(2)}) collective-permute-start(bf16[64,2048]{1,0:T(8,128)(2,1)S(1)} %add_convert_fusion.3), channel_id=1, source_target_pairs={{0,3},{1,0},{2,1},{3,2},{4,7},{5,4},{6,5},{7,6},{8,11},{9,8},{10,9... | collective-permute-start | bytes 786440 | tf_op jit(solution)/shard_map/ppermute | solution.py:27
  206.3 7.7 %collective-permute-start.19 = (bf16[64,2048]{1,0:T(8,128)(2,1)S(1)}, bf16[64,2048]{1,0:T(8,128)(2,1)S(1)}, u32[]{:S(2)}, u32[]{:S(2)}) collective-permute-start(bf16[64,2048]{1,0:T(8,128)(2,1)S(1)} %add_convert_fusion.4), channel_id=1, source_target_pairs={{0,1},{1,2},{2,3},{3,0},{4,5},{5,6},{6,7},{7,4},{8,9},{9,10},{10,1... | collective-permute-start | bytes 786440 | tf_op jit(solution)/shard_map/ppermute | solution.py:27
  207.1 21.5 %copy-start.19 = (f32[256]{0:T(256)S(1)}, f32[256]{0:T(256)}, u32[]{:S(2)}) copy-start(f32[256]{0:T(256)} %param.17) | copy-start | bytes 3076
  207.1 21.5 %copy-start.20 = (pred[256]{0:T(512)(128)(4,1)S(1)}, pred[256]{0:T(512)(128)(4,1)}, u32[]{:S(2)}) copy-start(pred[256]{0:T(512)(128)(4,1)} %get-tuple-element.70) | copy-start | bytes 772
  207.1 21.5 %copy-start.21 = (pred[256]{0:T(512)(128)(4,1)S(1)}, pred[256]{0:T(512)(128)(4,1)}, u32[]{:S(2)}) copy-start(pred[256]{0:T(512)(128)(4,1)} %get-tuple-element.71) | copy-start | bytes 772
  207.1 2.1 collective-permute-start.3
  209.3 4.7 %copy-start.8 = (bf16[64,2048]{1,0:T(8,128)(2,1)}, bf16[64,2048]{1,0:T(8,128)(2,1)S(1)}, u32[]{:S(2)}) copy-start(bf16[64,2048]{1,0:T(8,128)(2,1)S(1)} %collective-permute-done.20.refs_1_) | copy-start | bytes 786436
  217.1 44.5 %all-to-all-start.2 = ((bf16[16,8,2048]{2,1,0:T(8,128)(2,1)}), bf16[16,8,2048]{2,1,0:T(8,128)(2,1)S(1)}, u32[]{:S(2)}, u32[]{:S(2)}) async-start(bf16[16,8,2048]{2,1,0:T(8,128)(2,1)} %bitcast.77), calls=%async_computation.2 | async-start | bytes 1048576 | tf_op jit(solution)/shard_map/all_to_all | solution.py:93
  234.5 22.3 %collective-permute-start.11 = (bf16[128,2048]{1,0:T(8,128)(2,1)S(1)}, bf16[128,2048]{1,0:T(8,128)(2,1)S(1)}, u32[]{:S(2)}, u32[]{:S(2)}) collective-permute-start(bf16[128,2048]{1,0:T(8,128)(2,1)S(1)} %get-tuple-element.31), channel_id=1, source_target_pairs={{0,3},{1,0},{2,1},{3,2},{4,7},{5,4},{6,5},{7,6},{8,11},{9,8},{10,9... | collective-permute-start | bytes 1572872 | tf_op jit(solution)/shard_map/ppermute | solution.py:27
  237.3 22.9 %collective-permute-start.12 = (bf16[128,2048]{1,0:T(8,128)(2,1)S(1)}, bf16[128,2048]{1,0:T(8,128)(2,1)S(1)}, u32[]{:S(2)}, u32[]{:S(2)}) collective-permute-start(bf16[128,2048]{1,0:T(8,128)(2,1)S(1)} %get-tuple-element.32), channel_id=1, source_target_pairs={{0,1},{1,2},{2,3},{3,0},{4,5},{5,6},{6,7},{7,4},{8,9},{9,10},{10,1... | collective-permute-start | bytes 1572872 | tf_op jit(solution)/shard_map/ppermute | solution.py:27
  237.3 22.9 %collective-permute-start.13 = (bf16[128,2048]{1,0:T(8,128)(2,1)S(1)}, bf16[128,2048]{1,0:T(8,128)(2,1)S(1)}, u32[]{:S(2)}, u32[]{:S(2)}) collective-permute-start(bf16[128,2048]{1,0:T(8,128)(2,1)S(1)} %get-tuple-element.33), channel_id=1, source_target_pairs={{0,2},{1,3},{2,0},{3,1},{4,6},{5,7},{6,4},{7,5},{8,10},{9,11},{10,... | collective-permute-start | bytes 1572872 | tf_op jit(solution)/shard_map/ppermute | solution.py:27
  (8 other events, 15.1 us)
where the time goes:
time: 264 us; the launch traced here: 263 us
  waiting for transfers between devices  104 us (39%)
  starting transfers between devices  90.8 us (34%)
  Pallas kernels  34.5 us (13%)
  other arithmetic  12.7 us (5%)
  matrix products  10.8 us (4%)
  local copies, waits for them, and re-layouts  8.48 us (3%)
    ppermute x26, waiting for transfers between devices, turned(): lax.ppermute(value, axis, [(i, (i + by) % peers) for i in range(peers)])  68.3 us
    all_to_all x4, starting transfers between devices, same_core(): lax.all_to_all(value, 'ep', 0, 0, axis_index_groups=rings, tiled=True)  53.9 us
    all_to_all x4, waiting for transfers between devices, same_core(): lax.all_to_all(value, 'ep', 0, 0, axis_index_groups=rings, tiled=True)  35.1 us
    ppermute x26, starting transfers between devices, turned(): lax.ppermute(value, axis, [(i, (i + by) % peers) for i in range(peers)])  35.1 us
    pallas_call x2, Pallas kernels, expert_rows(): pl.pallas_call(expert_kernel(in_counts, out_counts, holders, local_expert...  29.8 us
  transfers between devices with their start and end apart: 34, of which 15 were waited for; matrix products, arithmetic and copies ran while one was open for 8% of the time, Pallas kernels for 13%

commit v1 on v0

--- a/solution.py
+++ b/solution.py
@@ -341,7 +341,7 @@
     back = []
     for k in range(chunks):
         arrived = same_core(outgoing[k], holders).reshape(-1, model_width + extra)
-        rows = ring_gather(arrived)
+        rows = ring_gather(arrived) if k + 1 < chunks else spread(arrived)
         count = arrived.shape[0]
         half = count // 2
         partials.append(expert_rows(rows, [count] + [half] * 6, sets))
@@ -361,13 +361,14 @@
     pooled = pool_mix(
         projected, pool_weight, pool_scale, windows, ep_index * projected.shape[0]
     )
-    product = jnp.dot(pooled, proj_out, preferred_element_type=jnp.float32).astype(jnp.bfloat16)
+    product = jnp.dot(pooled, proj_out, preferred_element_type=jnp.float32).astype(
+        jnp.bfloat16
+    )
     product = product.reshape(tp_count, own_count, model_width)
     parts = [
         lax.dynamic_index_in_dim(product, (tp_index - s) % tp_count, 0, keepdims=False)
         for s in [0] + tp_steps()
     ]
-    parts, _ = lax.optimization_barrier((parts, partials[-1][0]))
     mixed_rows = collect(parts)
 
     total = None

time: 264 us -> 276 us (1.045)
  starting transfers between devices: 90.8 us -> 103 us
    ppermute x26 -> x25, waiting for transfers between devices: 68.3 us -> 56.4 us  [turned(): lax.ppermute(value, axis, [(i, (i + by) % peers) for i in range(peers)])]
    all_to_all x4, waiting for transfers between devices: 35.1 us -> 45.7 us  [same_core(): lax.all_to_all(value, 'ep', 0, 0, axis_index_groups=rings, tiled=True)]
    ppermute x26 -> x25, starting transfers between devices: 35.1 us -> 45.1 us  [turned(): lax.ppermute(value, axis, [(i, (i + by) % peers) for i in range(peers)])]
  transfers between devices with their start and end apart: 34 -> 33, of which waited for: 15 -> 15; matrix products, arithmetic and copies ran while one was open for 8% -> 9% of each run, Pallas kernels for 13% -> 13%
where the time goes in v1:
time: 276 us; the launch traced here: 275 us
  starting transfers between devices  103 us (37%)
  waiting for transfers between devices  103 us (37%)
  Pallas kernels  34.5 us (12%)
  other arithmetic  15.4 us (6%)
  matrix products  10.8 us (4%)
  local copies, waits for them, and re-layouts  7 us (3%)
    ppermute x25, waiting for transfers between devices, turned(): lax.ppermute(value, axis, [(i, (i + by) % peers) for i in range(peers)])  56.4 us
    all_to_all x4, starting transfers between devices, same_core(): lax.all_to_all(value, 'ep', 0, 0, axis_index_groups=rings, tiled=True)  55.9 us
    all_to_all x4, waiting for transfers between devices, same_core(): lax.all_to_all(value, 'ep', 0, 0, axis_index_groups=rings, tiled=True)  45.7 us
    ppermute x25, starting transfers between devices, turned(): lax.ppermute(value, axis, [(i, (i + by) % peers) for i in range(peers)])  45.1 us
    pallas_call x2, Pallas kernels, expert_rows(): pl.pallas_call(expert_kernel(in_counts, out_counts, holders, local_expert...  29.8 us
  transfers between devices with their start and end apart: 33, of which 15 were waited for; matrix products, arithmetic and copies ran while one was open for 9% of the time, Pallas kernels for 13%

profile of v1, /device:TPU:40, one launch (start us, length us, event | category | flops | bytes accessed | tf_op | source)
XLA Modules:
  0.0 274.6 jit_solution(2981062895393534331)
XLA Ops:
  2.5 1.2 convert_reduce_fusion.1
  3.7 1.3 fusion.12
  5.0 1.4 fusion.14
  6.6 1.2 fusion.1
  7.8 24.1 %all-to-all-start.2 = ((bf16[16,8,2176]{2,1,0:T(8,128)(2,1)}), bf16[16,8,2176]{2,1,0:T(8,128)(2,1)S(1)}, u32[]{:S(2)}, u32[]{:S(2)}) async-start(bf16[16,8,2176]{2,1,0:T(8,128)(2,1)} %fusion.1), calls=%async_computation.2 | async-start | bytes 1114112 | tf_op jit(solution)/shard_map/all_to_all | solution.py:93
  33.7 28.0 %all-to-all-done.2 = bf16[16,8,2176]{2,1,0:T(8,128)(2,1)S(1)} async-done(((bf16[16,8,2176]{2,1,0:T(8,128)(2,1)}), bf16[16,8,2176]{2,1,0:T(8,128)(2,1)S(1)}, u32[]{:S(2)}, u32[]{:S(2)}) %all-to-all-start.2) | async-done | bytes 557088 | tf_op jit(solution)/shard_map/all_to_all | solution.py:93
  61.6 7.1 %all-to-all-start = ((bf16[16,8,2176]{2,1,0:T(8,128)(2,1)}), bf16[16,8,2176]{2,1,0:T(8,128)(2,1)S(1)}, u32[]{:S(2)}, u32[]{:S(2)}) async-start(bf16[16,8,2176]{2,1,0:T(8,128)(2,1)} %fusion), calls=%async_computation | async-start | bytes 1114112 | tf_op jit(solution)/shard_map/all_to_all | solution.py:93
  70.8 1.7 collective-permute-start.20
  72.5 1.7 collective-permute-start.21
  74.2 2.0 collective-permute-start.22
  76.8 1.2 fusion.11
  79.0 1.8 collective-permute-start.2
  80.8 17.8 %all-to-all-done = bf16[16,8,2176]{2,1,0:T(8,128)(2,1)S(1)} async-done(((bf16[16,8,2176]{2,1,0:T(8,128)(2,1)}), bf16[16,8,2176]{2,1,0:T(8,128)(2,1)S(1)}, u32[]{:S(2)}, u32[]{:S(2)}) %all-to-all-start) | async-done | bytes 557088 | tf_op jit(solution)/shard_map/all_to_all | solution.py:93
  98.6 3.2 %collective-permute-start.8 = (bf16[128,2176]{1,0:T(8,128)(2,1)S(1)}, bf16[128,2176]{1,0:T(8,128)(2,1)}, u32[]{:S(2)}, u32[]{:S(2)}) collective-permute-start(bf16[128,2176]{1,0:T(8,128)(2,1)S(1)} %bitcast.82), channel_id=1, source_target_pairs={{0,3},{1,0},{2,1},{3,2},{4,7},{5,4},{6,5},{7,6},{8,11},{9,8},{10,9... | collective-permute-start | bytes 1671176 | tf_op jit(solution)/shard_map/ppermute | solution.py:27
  101.7 14.9 %experts.3 = (bf16[128,2048]{1,0:T(8,128)(2,1)}, bf16[64,2048]{1,0:T(8,128)(2,1)}, bf16[64,2048]{1,0:T(8,128)(2,1)}, bf16[64,2048]{1,0:T(8,128)(2,1)}, bf16[64,2...) custom-call(bf16[128,2176]{1,0:T(8,128)(2,1)} %bitcast.88, ...), custom_call_target="tpu_custom_call" | custom-call | flops 6442450944 | bytes 16908288 | tf_op jit(solution)/shard_map/experts/pallas_call | solution.py:238
  116.7 9.8 %collective-permute-start.27 = (bf16[64,2048]{1,0:T(8,128)(2,1)}, bf16[64,2048]{1,0:T(8,128)(2,1)S(1)}, u32[]{:S(2)}, u32[]{:S(2)}) collective-permute-start(bf16[64,2048]{1,0:T(8,128)(2,1)} %get-tuple-element.39), channel_id=1, source_target_pairs={{0,3},{1,0},{2,1},{3,2},{4,7},{5,4},{6,5},{7,6},{8,11},{9,8},{10,9... | collective-permute-start | bytes 786440 | tf_op jit(solution)/shard_map/ppermute | solution.py:27
  126.5 8.0 %collective-permute-done.8.refs_2_ = bf16[128,2176]{1,0:T(8,128)(2,1)} collective-permute-done((bf16[128,2176]{1,0:T(8,128)(2,1)S(1)}, bf16[128,2176]{1,0:T(8,128)(2,1)}, u32[]{:S(2)}, u32[]{:S(2)}) %collective-permute-start.8) | collective-permute-done | bytes 557088 | tf_op jit(solution)/shard_map/ppermute | solution.py:27
  134.5 1.5 collective-permute-start
  137.1 1.8 collective-permute-start.10
  140.1 1.5 collective-permute-start.23
  142.6 1.5 collective-permute-start.9
  144.2 12.2 %collective-permute-done.23 = bf16[64,2048]{1,0:T(8,128)(2,1)S(1)} collective-permute-done((bf16[64,2048]{1,0:T(8,128)(2,1)}, bf16[64,2048]{1,0:T(8,128)(2,1)S(1)}, u32[]{:S(2)}, u32[]{:S(2)}) %collective-permute-start.23) | collective-permute-done | bytes 262176 | tf_op jit(solution)/shard_map/ppermute | solution.py:27
  156.4 1.6 collective-permute-start.25
  158.6 2.8 %collective-permute-start.28 = (bf16[64,2048]{1,0:T(8,128)(2,1)S(1)}, bf16[64,2048]{1,0:T(8,128)(2,1)S(1)}, u32[]{:S(2)}, u32[]{:S(2)}) collective-permute-start(bf16[64,2048]{1,0:T(8,128)(2,1)S(1)} %add_convert_fusion), channel_id=1, source_target_pairs={{0,3},{1,0},{2,1},{3,2},{4,7},{5,4},{6,5},{7,6},{8,11},{9,8},{10,9... | collective-permute-start | bytes 786440 | tf_op jit(solution)/shard_map/ppermute | solution.py:27
  161.4 1.5 collective-permute-done.25.refs_1_
  163.3 2.6 pad_maximum_fusion
  165.9 1.3 collective-permute-done.26.refs_2_
  167.2 3.3 %collective-permute-done.24.refs_0_ = bf16[64,2048]{1,0:T(8,128)(2,1)S(1)} collective-permute-done((bf16[64,2048]{1,0:T(8,128)(2,1)S(1)}, bf16[64,2048]{1,0:T(8,128)(2,1)S(1)}, u32[]{:S(2)}, u32[]{:S(2)}) %collective-permute-start.24) | collective-permute-done | bytes 262176 | tf_op jit(solution)/shard_map/ppermute | solution.py:27
  171.3 2.3 add_halves.3
  173.6 12.0 %all-to-all-start.3 = ((bf16[16,8,2048]{2,1,0:T(8,128)(2,1)}), bf16[16,8,2048]{2,1,0:T(8,128)(2,1)S(1)}, u32[]{:S(2)}, u32[]{:S(2)}) async-start(bf16[16,8,2048]{2,1,0:T(8,128)(2,1)} %bitcast.78), calls=%async_computation.3 | async-start | bytes 1048576 | tf_op jit(solution)/shard_map/all_to_all | solution.py:93
  185.6 14.9 %experts.2 = (bf16[128,2048]{1,0:T(8,128)(2,1)}, bf16[64,2048]{1,0:T(8,128)(2,1)}, bf16[64,2048]{1,0:T(8,128)(2,1)}, bf16[64,2048]{1,0:T(8,128)(2,1)}, bf16[64,2...) custom-call(bf16[128,2176]{1,0:T(8,128)(2,1)} %bitcast.84, ...), custom_call_target="tpu_custom_call" | custom-call | flops 6442450944 | bytes 16908288 | tf_op jit(solution)/shard_map/experts/pallas_call | solution.py:238
  200.6 1.7 collective-permute-start.18
  202.3 2.6 convolution_convert_fusion.3
  205.5 2.8 %collective-permute-start.16 = (bf16[64,2048]{1,0:T(8,128)(2,1)}, bf16[64,2048]{1,0:T(8,128)(2,1)S(1)}, u32[]{:S(2)}, u32[]{:S(2)}) collective-permute-start(bf16[64,2048]{1,0:T(8,128)(2,1)} %get-tuple-element.29), channel_id=1, source_target_pairs={{0,3},{1,0},{2,1},{3,2},{4,7},{5,4},{6,5},{7,6},{8,11},{9,8},{10,9... | collective-permute-start | bytes 786440 | tf_op jit(solution)/shard_map/ppermute | solution.py:27
  208.3 1.8 collective-permute-done.18
  210.1 2.9 %collective-permute-start.19 = (bf16[64,2048]{1,0:T(8,128)(2,1)S(1)}, bf16[64,2048]{1,0:T(8,128)(2,1)}, u32[]{:S(2)}, u32[]{:S(2)}) collective-permute-start(bf16[64,2048]{1,0:T(8,128)(2,1)S(1)} %add_convert_fusion.2), channel_id=1, source_target_pairs={{0,3},{1,0},{2,1},{3,2},{4,7},{5,4},{6,5},{7,6},{8,11},{9,8},{10,9... | collective-permute-start | bytes 786440 | tf_op jit(solution)/shard_map/ppermute | solution.py:27
  213.0 1.8 collective-permute-done.14
  215.7 1.3 collective-permute-start.3
  218.4 4.2 %collective-permute-done.15.refs_0_ = bf16[64,2048]{1,0:T(8,128)(2,1)S(1)} collective-permute-done((bf16[64,2048]{1,0:T(8,128)(2,1)S(1)}, bf16[64,2048]{1,0:T(8,128)(2,1)S(1)}, u32[]{:S(2)}, u32[]{:S(2)}) %collective-permute-start.15) | collective-permute-done | bytes 262176 | tf_op jit(solution)/shard_map/ppermute | solution.py:27
  223.3 2.3 add_halves.2
  225.7 12.6 %all-to-all-start.1 = ((bf16[16,8,2048]{2,1,0:T(8,128)(2,1)}), bf16[16,8,2048]{2,1,0:T(8,128)(2,1)S(1)}, u32[]{:S(2)}, u32[]{:S(2)}) async-start(bf16[16,8,2048]{2,1,0:T(8,128)(2,1)} %bitcast.79), calls=%async_computation.1 | async-start | bytes 1048576 | tf_op jit(solution)/shard_map/all_to_all | solution.py:93
  238.4 4.2 %convolution_convert_fusion.2 = bf16[512,2048]{1,0:T(8,128)(2,1)} fusion(bf16[256,2048]{1,0:T(8,128)(2,1)S(1)} %copy-done, f32[256]{0:T(256)S(1)} %copy-done.16, f32[527,256]{1,0:T(8,128)S(1)} %maximum_convert_fusion, s32[256]{0:T(256)S(1)} %fusion.82, s32[512]{0:T(512)S(1)} %add_add_fusion, pred[256]{0:T(512)(128)(4,1)S(1)} %get-tuple-element.53, ...), kind=kOutput, calls=%fused_computation.5 | convolution fusion | flops 609878016 | bytes 11677184 | tf_op jit(solution)/shard_map/dot_general | solution.py:364
  242.6 2.3 dynamic-slice_bitcast_fusion.2
  244.9 2.7 collective-permute-start.4
  247.6 1.5 collective-permute-start.6
  249.1 18.3 %collective-permute-done.4 = bf16[128,2048]{1,0:T(8,128)(2,1)} collective-permute-done((bf16[128,2048]{1,0:T(8,128)(2,1)}, bf16[128,2048]{1,0:T(8,128)(2,1)}, u32[]{:S(2)}, u32[]{:S(2)}) %collective-permute-start.4) | collective-permute-done | bytes 524320 | tf_op jit(solution)/shard_map/ppermute | solution.py:27
  267.4 3.2 %collective-permute-done.5 = bf16[128,2048]{1,0:T(8,128)(2,1)} collective-permute-done((bf16[128,2048]{1,0:T(8,128)(2,1)S(1)}, bf16[128,2048]{1,0:T(8,128)(2,1)}, u32[]{:S(2)}, u32[]{:S(2)}) %collective-permute-start.5) | collective-permute-done | bytes 524320 | tf_op jit(solution)/shard_map/ppermute | solution.py:27
  270.6 2.6 fusion.17
  (120 shorter events, 16.9 us)
Async XLA Ops:
  0.6 237.7 %copy-start = (bf16[256,2048]{1,0:T(8,128)(2,1)S(1)}, bf16[256,2048]{1,0:T(8,128)(2,1)}, u32[]{:S(2)}) copy-start(bf16[256,2048]{1,0:T(8,128)(2,1)} %param.18) | copy-start | bytes 3145732
  6.6 63.4 %copy-start.1 = (bf16[128,2048]{1,0:T(8,128)(2,1)S(1)}, bf16[128,2048]{1,0:T(8,128)(2,1)}, u32[]{:S(2)}) copy-start(bf16[128,2048]{1,0:T(8,128)(2,1)} %param.13) | copy-start | bytes 1572868
  7.8 62.6 %copy-start.13 = (f32[2048]{0:T(1024)S(1)}, f32[2048]{0:T(1024)}, u32[]{:S(2)}) copy-start(f32[2048]{0:T(1024)} %param.14) | copy-start | bytes 24580
  7.8 53.8 %all-to-all-start.2 = ((bf16[16,8,2176]{2,1,0:T(8,128)(2,1)}), bf16[16,8,2176]{2,1,0:T(8,128)(2,1)S(1)}, u32[]{:S(2)}, u32[]{:S(2)}) async-start(bf16[16,8,2176]{2,1,0:T(8,128)(2,1)} %fusion.1), calls=%async_computation.2 | async-start | bytes 1114112 | tf_op jit(solution)/shard_map/all_to_all | solution.py:93
  33.1 41.1 %collective-permute-start.11 = (bf16[2,2048,256]{2,1,0:T(8,128)(2,1)}, bf16[2,2048,256]{2,1,0:T(8,128)(2,1)}, u32[]{:S(2)}, u32[]{:S(2)}) collective-permute-start(bf16[2,2048,256]{2,1,0:T(8,128)(2,1)} %refs_4_), channel_id=1, source_target_pairs={{0,4},{4,0},{8,12},{12,8},{16,20},{20,16},{24,28},{28,24},{32,36},... | collective-permute-start | bytes 6291464 | tf_op jit(solution)/shard_map/ppermute | solution.py:333
  33.1 44.9 %collective-permute-start.12 = (bf16[2,2048,256]{2,1,0:T(8,128)(2,1)}, bf16[2,2048,256]{2,1,0:T(8,128)(2,1)}, u32[]{:S(2)}, u32[]{:S(2)}) collective-permute-start(bf16[2,2048,256]{2,1,0:T(8,128)(2,1)} %refs_5_.1), channel_id=1, source_target_pairs={{0,4},{4,0},{8,12},{12,8},{16,20},{20,16},{24,28},{28,24},{32,36},... | collective-permute-start | bytes 6291464 | tf_op jit(solution)/shard_map/ppermute | solution.py:333
  33.6 45.4 %collective-permute-start.13 = (bf16[2,256,2048]{2,1,0:T(8,128)(2,1)}, bf16[2,256,2048]{2,1,0:T(8,128)(2,1)}, u32[]{:S(2)}, u32[]{:S(2)}) collective-permute-start(bf16[2,256,2048]{2,1,0:T(8,128)(2,1)} %refs_6_.1), channel_id=1, source_target_pairs={{0,4},{4,0},{8,12},{12,8},{16,20},{20,16},{24,28},{28,24},{32,36},... | collective-permute-start | bytes 6291464 | tf_op jit(solution)/shard_map/ppermute | solution.py:333
  61.6 16.3 %copy-start.3 = (bf16[16,8,2176]{2,1,0:T(8,128)(2,1)}, bf16[16,8,2176]{2,1,0:T(8,128)(2,1)S(1)}, u32[]{:S(2)}) copy-start(bf16[16,8,2176]{2,1,0:T(8,128)(2,1)S(1)} %all-to-all-done.2) | copy-start | bytes 1671172
  61.6 36.9 %all-to-all-start = ((bf16[16,8,2176]{2,1,0:T(8,128)(2,1)}), bf16[16,8,2176]{2,1,0:T(8,128)(2,1)S(1)}, u32[]{:S(2)}, u32[]{:S(2)}) async-start(bf16[16,8,2176]{2,1,0:T(8,128)(2,1)} %fusion), calls=%async_computation | async-start | bytes 1114112 | tf_op jit(solution)/shard_map/all_to_all | solution.py:93
  70.8 27.8 %collective-permute-start.20 = (bf16[128,2176]{1,0:T(8,128)(2,1)S(1)}, bf16[128,2176]{1,0:T(8,128)(2,1)}, u32[]{:S(2)}, u32[]{:S(2)}) collective-permute-start(bf16[128,2176]{1,0:T(8,128)(2,1)S(1)} %bitcast.85), channel_id=1, source_target_pairs={{0,1},{1,2},{2,3},{3,0},{4,5},{5,6},{6,7},{7,4},{8,9},{9,10},{10,1... | collective-permute-start | bytes 1671176 | tf_op jit(solution)/shard_map/ppermute | solution.py:27
  72.5 29.2 %collective-permute-start.21 = (bf16[128,2176]{1,0:T(8,128)(2,1)S(1)}, bf16[128,2176]{1,0:T(8,128)(2,1)}, u32[]{:S(2)}, u32[]{:S(2)}) collective-permute-start(bf16[128,2176]{1,0:T(8,128)(2,1)S(1)} %bitcast.86), channel_id=1, source_target_pairs={{0,3},{1,0},{2,1},{3,2},{4,7},{5,4},{6,5},{7,6},{8,11},{9,8},{10,9... | collective-permute-start | bytes 1671176 | tf_op jit(solution)/shard_map/ppermute | solution.py:27
  74.2 27.5 %collective-permute-start.22 = (bf16[128,2176]{1,0:T(8,128)(2,1)S(1)}, bf16[128,2176]{1,0:T(8,128)(2,1)}, u32[]{:S(2)}, u32[]{:S(2)}) collective-permute-start(bf16[128,2176]{1,0:T(8,128)(2,1)S(1)} %bitcast.87), channel_id=1, source_target_pairs={{0,2},{1,3},{2,0},{3,1},{4,6},{5,7},{6,4},{7,5},{8,10},{9,11},{10,... | collective-permute-start | bytes 1671176 | tf_op jit(solution)/shard_map/ppermute | solution.py:27
  78.0 64.6 %collective-permute-start.1 = (bf16[128,2048]{1,0:T(8,128)(2,1)}, bf16[128,2048]{1,0:T(8,128)(2,1)S(1)}, u32[]{:S(2)}, u32[]{:S(2)}) collective-permute-start(bf16[128,2048]{1,0:T(8,128)(2,1)} %fusion.11), channel_id=1, source_target_pairs={{0,3},{1,0},{2,1},{3,2},{4,7},{5,4},{6,5},{7,6},{8,11},{9,8},{10,9... | collective-permute-start | bytes 1572872 | tf_op jit(solution)/shard_map/ppermute | solution.py:27
  79.0 79.0 %collective-permute-start.2 = (bf16[128,2048]{1,0:T(8,128)(2,1)}, bf16[128,2048]{1,0:T(8,128)(2,1)}, u32[]{:S(2)}, u32[]{:S(2)}) collective-permute-start(bf16[128,2048]{1,0:T(8,128)(2,1)} %fusion.11), channel_id=1, source_target_pairs={{0,2},{1,3},{2,0},{3,1},{4,6},{5,7},{6,4},{7,5},{8,10},{9,11},{10,... | collective-permute-start | bytes 1572872 | tf_op jit(solution)/shard_map/ppermute | solution.py:27
  98.5 18.1 %copy-start.2 = (bf16[16,8,2176]{2,1,0:T(8,128)(2,1)}, bf16[16,8,2176]{2,1,0:T(8,128)(2,1)S(1)}, u32[]{:S(2)}) copy-start(bf16[16,8,2176]{2,1,0:T(8,128)(2,1)S(1)} %all-to-all-done) | copy-start | bytes 1671172
  98.6 36.0 %collective-permute-start.8 = (bf16[128,2176]{1,0:T(8,128)(2,1)S(1)}, bf16[128,2176]{1,0:T(8,128)(2,1)}, u32[]{:S(2)}, u32[]{:S(2)}) collective-permute-start(bf16[128,2176]{1,0:T(8,128)(2,1)S(1)} %bitcast.82), channel_id=1, source_target_pairs={{0,3},{1,0},{2,1},{3,2},{4,7},{5,4},{6,5},{7,6},{8,11},{9,8},{10,9... | collective-permute-start | bytes 1671176 | tf_op jit(solution)/shard_map/ppermute | solution.py:27
  101.7 35.3 %collective-permute-start.7 = (bf16[128,2176]{1,0:T(8,128)(2,1)S(1)}, bf16[128,2176]{1,0:T(8,128)(2,1)}, u32[]{:S(2)}, u32[]{:S(2)}) collective-permute-start(bf16[128,2176]{1,0:T(8,128)(2,1)S(1)} %bitcast.83), channel_id=1, source_target_pairs={{0,1},{1,2},{2,3},{3,0},{4,5},{5,6},{6,7},{7,4},{8,9},{9,10},{10,1... | collective-permute-start | bytes 1671176 | tf_op jit(solution)/shard_map/ppermute | solution.py:27
  116.7 41.3 %copy-start.4 = (bf16[64,2048]{1,0:T(8,128)(2,1)S(1)}, bf16[64,2048]{1,0:T(8,128)(2,1)}, u32[]{:S(2)}) copy-start(bf16[64,2048]{1,0:T(8,128)(2,1)} %get-tuple-element.34) | copy-start | bytes 786436
  116.7 41.4 %copy-start.14 = (bf16[64,2048]{1,0:T(8,128)(2,1)S(1)}, bf16[64,2048]{1,0:T(8,128)(2,1)}, u32[]{:S(2)}) copy-start(bf16[64,2048]{1,0:T(8,128)(2,1)} %get-tuple-element.37) | copy-start | bytes 786436
  116.7 23.4 %collective-permute-start.27 = (bf16[64,2048]{1,0:T(8,128)(2,1)}, bf16[64,2048]{1,0:T(8,128)(2,1)S(1)}, u32[]{:S(2)}, u32[]{:S(2)}) collective-permute-start(bf16[64,2048]{1,0:T(8,128)(2,1)} %get-tuple-element.39), channel_id=1, source_target_pairs={{0,3},{1,0},{2,1},{3,2},{4,7},{5,4},{6,5},{7,6},{8,11},{9,8},{10,9... | collective-permute-start | bytes 786440 | tf_op jit(solution)/shard_map/ppermute | solution.py:27
  134.5 24.1 %collective-permute-start = (bf16[128,2048]{1,0:T(8,128)(2,1)}, bf16[128,2048]{1,0:T(8,128)(2,1)S(1)}, u32[]{:S(2)}, u32[]{:S(2)}) collective-permute-start(bf16[128,2048]{1,0:T(8,128)(2,1)} %fusion.11), channel_id=1, source_target_pairs={{0,1},{1,2},{2,3},{3,0},{4,5},{5,6},{6,7},{7,4},{8,9},{9,10},{10,1... | collective-permute-start | bytes 1572872 | tf_op jit(solution)/shard_map/ppermute | solution.py:27
  137.1 48.6 %collective-permute-start.10 = (bf16[64,2176]{1,0:T(8,128)(2,1)S(1)}, bf16[64,2176]{1,0:T(8,128)(2,1)}, u32[]{:S(2)}, u32[]{:S(2)}) collective-permute-start(bf16[64,2176]{1,0:T(8,128)(2,1)S(1)} %slice.163), channel_id=1, source_target_pairs={{0,3},{1,0},{2,1},{3,2},{4,7},{5,4},{6,5},{7,6},{8,11},{9,8},{10,9... | collective-permute-start | bytes 835592 | tf_op jit(solution)/shard_map/ppermute | solution.py:27
  140.1 16.3 %collective-permute-start.23 = (bf16[64,2048]{1,0:T(8,128)(2,1)}, bf16[64,2048]{1,0:T(8,128)(2,1)S(1)}, u32[]{:S(2)}, u32[]{:S(2)}) collective-permute-start(bf16[64,2048]{1,0:T(8,128)(2,1)} %get-tuple-element.35), channel_id=1, source_target_pairs={{0,1},{1,2},{2,3},{3,0},{4,5},{5,6},{6,7},{7,4},{8,9},{9,10},{10,1... | collective-permute-start | bytes 786440 | tf_op jit(solution)/shard_map/ppermute | solution.py:27
  142.6 43.0 %collective-permute-start.9 = (bf16[64,2176]{1,0:T(8,128)(2,1)S(1)}, bf16[64,2176]{1,0:T(8,128)(2,1)}, u32[]{:S(2)}, u32[]{:S(2)}) collective-permute-start(bf16[64,2176]{1,0:T(8,128)(2,1)S(1)} %slice.162), channel_id=1, source_target_pairs={{0,1},{1,2},{2,3},{3,0},{4,5},{5,6},{6,7},{7,4},{8,9},{9,10},{10,1... | collective-permute-start | bytes 835592 | tf_op jit(solution)/shard_map/ppermute | solution.py:27
  156.4 6.6 %collective-permute-start.25 = (bf16[64,2048]{1,0:T(8,128)(2,1)}, bf16[64,2048]{1,0:T(8,128)(2,1)S(1)}, u32[]{:S(2)}, u32[]{:S(2)}) collective-permute-start(bf16[64,2048]{1,0:T(8,128)(2,1)} %get-tuple-element.36), channel_id=1, source_target_pairs={{0,3},{1,0},{2,1},{3,2},{4,7},{5,4},{6,5},{7,6},{8,11},{9,8},{10,9... | collective-permute-start | bytes 786440 | tf_op jit(solution)/shard_map/ppermute | solution.py:27
  158.1 9.2 %collective-permute-start.26 = (bf16[64,2048]{1,0:T(8,128)(2,1)S(1)}, bf16[64,2048]{1,0:T(8,128)(2,1)S(1)}, u32[]{:S(2)}, u32[]{:S(2)}) collective-permute-start(bf16[64,2048]{1,0:T(8,128)(2,1)S(1)} %copy-done.14), channel_id=1, source_target_pairs={{0,1},{1,2},{2,3},{3,0},{4,5},{5,6},{6,7},{7,4},{8,9},{9,10},{10,1... | collective-permute-start | bytes 786440 | tf_op jit(solution)/shard_map/ppermute | solution.py:27
  158.6 8.6 %collective-permute-start.28 = (bf16[64,2048]{1,0:T(8,128)(2,1)S(1)}, bf16[64,2048]{1,0:T(8,128)(2,1)S(1)}, u32[]{:S(2)}, u32[]{:S(2)}) collective-permute-start(bf16[64,2048]{1,0:T(8,128)(2,1)S(1)} %add_convert_fusion), channel_id=1, source_target_pairs={{0,3},{1,0},{2,1},{3,2},{4,7},{5,4},{6,5},{7,6},{8,11},{9,8},{10,9... | collective-permute-start | bytes 786440 | tf_op jit(solution)/shard_map/ppermute | solution.py:27
  163.0 7.6 %collective-permute-start.24 = (bf16[64,2048]{1,0:T(8,128)(2,1)S(1)}, bf16[64,2048]{1,0:T(8,128)(2,1)S(1)}, u32[]{:S(2)}, u32[]{:S(2)}) collective-permute-start(bf16[64,2048]{1,0:T(8,128)(2,1)S(1)} %add_convert_fusion.1), channel_id=1, source_target_pairs={{0,1},{1,2},{2,3},{3,0},{4,5},{5,6},{6,7},{7,4},{8,9},{9,10},{10,1... | collective-permute-start | bytes 786440 | tf_op jit(solution)/shard_map/ppermute | solution.py:27
  173.6 52.1 %all-to-all-start.3 = ((bf16[16,8,2048]{2,1,0:T(8,128)(2,1)}), bf16[16,8,2048]{2,1,0:T(8,128)(2,1)S(1)}, u32[]{:S(2)}, u32[]{:S(2)}) async-start(bf16[16,8,2048]{2,1,0:T(8,128)(2,1)} %bitcast.78), calls=%async_computation.3 | async-start | bytes 1048576 | tf_op jit(solution)/shard_map/all_to_all | solution.py:93
  200.6 9.5 %collective-permute-start.18 = (bf16[64,2048]{1,0:T(8,128)(2,1)}, bf16[64,2048]{1,0:T(8,128)(2,1)S(1)}, u32[]{:S(2)}, u32[]{:S(2)}) collective-permute-start(bf16[64,2048]{1,0:T(8,128)(2,1)} %get-tuple-element.32), channel_id=1, source_target_pairs={{0,3},{1,0},{2,1},{3,2},{4,7},{5,4},{6,5},{7,6},{8,11},{9,8},{10,9... | collective-permute-start | bytes 786440 | tf_op jit(solution)/shard_map/ppermute | solution.py:27
  202.3 7.8 %copy-start.6 = (bf16[64,2048]{1,0:T(8,128)(2,1)S(1)}, bf16[64,2048]{1,0:T(8,128)(2,1)}, u32[]{:S(2)}) copy-start(bf16[64,2048]{1,0:T(8,128)(2,1)} %get-tuple-element.31) | copy-start | bytes 786436
  202.3 12.6 %copy-start.5 = (bf16[64,2048]{1,0:T(8,128)(2,1)S(1)}, bf16[64,2048]{1,0:T(8,128)(2,1)}, u32[]{:S(2)}) copy-start(bf16[64,2048]{1,0:T(8,128)(2,1)} %get-tuple-element.27) | copy-start | bytes 786436
  204.9 9.9 %collective-permute-start.14 = (bf16[64,2048]{1,0:T(8,128)(2,1)S(1)}, bf16[64,2048]{1,0:T(8,128)(2,1)S(1)}, u32[]{:S(2)}, u32[]{:S(2)}) collective-permute-start(bf16[64,2048]{1,0:T(8,128)(2,1)S(1)} %copy-done.15), channel_id=1, source_target_pairs={{0,1},{1,2},{2,3},{3,0},{4,5},{5,6},{6,7},{7,4},{8,9},{9,10},{10,1... | collective-permute-start | bytes 786440 | tf_op jit(solution)/shard_map/ppermute | solution.py:27
  205.5 12.4 %collective-permute-start.16 = (bf16[64,2048]{1,0:T(8,128)(2,1)}, bf16[64,2048]{1,0:T(8,128)(2,1)S(1)}, u32[]{:S(2)}, u32[]{:S(2)}) collective-permute-start(bf16[64,2048]{1,0:T(8,128)(2,1)} %get-tuple-element.29), channel_id=1, source_target_pairs={{0,3},{1,0},{2,1},{3,2},{4,7},{5,4},{6,5},{7,6},{8,11},{9,8},{10,9... | collective-permute-start | bytes 786440 | tf_op jit(solution)/shard_map/ppermute | solution.py:27
  208.3 10.1 %collective-permute-start.17 = (bf16[64,2048]{1,0:T(8,128)(2,1)}, bf16[64,2048]{1,0:T(8,128)(2,1)}, u32[]{:S(2)}, u32[]{:S(2)}) collective-permute-start(bf16[64,2048]{1,0:T(8,128)(2,1)} %get-tuple-element.30), channel_id=1, source_target_pairs={{0,1},{1,2},{2,3},{3,0},{4,5},{5,6},{6,7},{7,4},{8,9},{9,10},{10,1... | collective-permute-start | bytes 786440 | tf_op jit(solution)/shard_map/ppermute | solution.py:27
  210.1 8.2 %collective-permute-start.19 = (bf16[64,2048]{1,0:T(8,128)(2,1)S(1)}, bf16[64,2048]{1,0:T(8,128)(2,1)}, u32[]{:S(2)}, u32[]{:S(2)}) collective-permute-start(bf16[64,2048]{1,0:T(8,128)(2,1)S(1)} %add_convert_fusion.2), channel_id=1, source_target_pairs={{0,3},{1,0},{2,1},{3,2},{4,7},{5,4},{6,5},{7,6},{8,11},{9,8},{10,9... | collective-permute-start | bytes 786440 | tf_op jit(solution)/shard_map/ppermute | solution.py:27
  214.9 7.7 %collective-permute-start.15 = (bf16[64,2048]{1,0:T(8,128)(2,1)S(1)}, bf16[64,2048]{1,0:T(8,128)(2,1)S(1)}, u32[]{:S(2)}, u32[]{:S(2)}) collective-permute-start(bf16[64,2048]{1,0:T(8,128)(2,1)S(1)} %add_convert_fusion.3), channel_id=1, source_target_pairs={{0,1},{1,2},{2,3},{3,0},{4,5},{5,6},{6,7},{7,4},{8,9},{9,10},{10,1... | collective-permute-start | bytes 786440 | tf_op jit(solution)/shard_map/ppermute | solution.py:27
  215.7 22.6 %copy-start.16 = (f32[256]{0:T(256)S(1)}, f32[256]{0:T(256)}, u32[]{:S(2)}) copy-start(f32[256]{0:T(256)} %param.17) | copy-start | bytes 3076
  215.7 22.6 %copy-start.17 = (pred[256]{0:T(512)(128)(4,1)S(1)}, pred[256]{0:T(512)(128)(4,1)}, u32[]{:S(2)}) copy-start(pred[256]{0:T(512)(128)(4,1)} %get-tuple-element.62) | copy-start | bytes 772
  215.7 22.6 %copy-start.18 = (pred[256]{0:T(512)(128)(4,1)S(1)}, pred[256]{0:T(512)(128)(4,1)}, u32[]{:S(2)}) copy-start(pred[256]{0:T(512)(128)(4,1)} %get-tuple-element.63) | copy-start | bytes 772
  215.7 22.6 %copy-start.19 = (pred[256]{0:T(512)(128)(4,1)S(1)}, pred[256]{0:T(512)(128)(4,1)}, u32[]{:S(2)}) copy-start(pred[256]{0:T(512)(128)(4,1)} %get-tuple-element.64) | copy-start | bytes 772
  215.7 22.6 %copy-start.20 = (pred[256]{0:T(512)(128)(4,1)S(1)}, pred[256]{0:T(512)(128)(4,1)}, u32[]{:S(2)}) copy-start(pred[256]{0:T(512)(128)(4,1)} %get-tuple-element.65) | copy-start | bytes 772
  215.7 22.6 %copy-start.21 = (pred[256]{0:T(512)(128)(4,1)S(1)}, pred[256]{0:T(512)(128)(4,1)}, u32[]{:S(2)}) copy-start(pred[256]{0:T(512)(128)(4,1)} %get-tuple-element.66) | copy-start | bytes 772
  215.7 2.1 collective-permute-start.3
  225.7 47.9 %all-to-all-start.1 = ((bf16[16,8,2048]{2,1,0:T(8,128)(2,1)}), bf16[16,8,2048]{2,1,0:T(8,128)(2,1)S(1)}, u32[]{:S(2)}, u32[]{:S(2)}) async-start(bf16[16,8,2048]{2,1,0:T(8,128)(2,1)} %bitcast.79), calls=%async_computation.1 | async-start | bytes 1048576 | tf_op jit(solution)/shard_map/all_to_all | solution.py:93
  244.9 22.5 %collective-permute-start.4 = (bf16[128,2048]{1,0:T(8,128)(2,1)}, bf16[128,2048]{1,0:T(8,128)(2,1)}, u32[]{:S(2)}, u32[]{:S(2)}) collective-permute-start(bf16[128,2048]{1,0:T(8,128)(2,1)} %get-tuple-element.42), channel_id=1, source_target_pairs={{0,3},{1,0},{2,1},{3,2},{4,7},{5,4},{6,5},{7,6},{8,11},{9,8},{10,9... | collective-permute-start | bytes 1572872 | tf_op jit(solution)/shard_map/ppermute | solution.py:27
  247.6 23.0 %collective-permute-start.5 = (bf16[128,2048]{1,0:T(8,128)(2,1)S(1)}, bf16[128,2048]{1,0:T(8,128)(2,1)}, u32[]{:S(2)}, u32[]{:S(2)}) collective-permute-start(bf16[128,2048]{1,0:T(8,128)(2,1)S(1)} %get-tuple-element.44), channel_id=1, source_target_pairs={{0,1},{1,2},{2,3},{3,0},{4,5},{5,6},{6,7},{7,4},{8,9},{9,10},{10,1... | collective-permute-start | bytes 1572872 | tf_op jit(solution)/shard_map/ppermute | solution.py:27
  247.6 23.0 %collective-permute-start.6 = (bf16[128,2048]{1,0:T(8,128)(2,1)S(1)}, bf16[128,2048]{1,0:T(8,128)(2,1)}, u32[]{:S(2)}, u32[]{:S(2)}) collective-permute-start(bf16[128,2048]{1,0:T(8,128)(2,1)S(1)} %get-tuple-element.43), channel_id=1, source_target_pairs={{0,2},{1,3},{2,0},{3,1},{4,6},{5,7},{6,4},{7,5},{8,10},{9,11},{10,... | collective-permute-start | bytes 1572872 | tf_op jit(solution)/shard_map/ppermute | solution.py:27
  (7 other events, 18.4 us)

commit v2 on v1

--- a/solution.py
+++ b/solution.py
@@ -91,15 +91,6 @@
     peers = lax.axis_size("ep")
     rings = [list(range(c, peers, holders)) for c in range(holders)]
     return lax.all_to_all(value, "ep", 0, 0, axis_index_groups=rings, tiled=True)
-
-
-def ring_gather(value):
-    half = value.shape[0] // 2
-    before = turned(value, "tp", 1)
-    after = turned(value, "tp", -1)
-    low = turned(before[:half], "tp", 1)
-    high = turned(after[half:], "tp", -1)
-    return [value, before, after, low, high]
 
 
 def add_halves(own, lows, highs):
@@ -341,7 +332,7 @@
     back = []
     for k in range(chunks):
         arrived = same_core(outgoing[k], holders).reshape(-1, model_width + extra)
-        rows = ring_gather(arrived) if k + 1 < chunks else spread(arrived)
+        rows = spread(arrived)
         count = arrived.shape[0]
         half = count // 2
         partials.append(expert_rows(rows, [count] + [half] * 6, sets))

time: 276 us -> 273 us (0.989)
  starting transfers between devices: 103 us -> 97.4 us
  waiting for transfers between devices: 103 us -> 106 us
    ppermute x25 -> x24, waiting for transfers between devices: 56.4 us -> 77.7 us  [turned(): lax.ppermute(value, axis, [(i, (i + by) % peers) for i in range(peers)])]
    all_to_all x4, waiting for transfers between devices: 45.7 us -> 27.5 us  [same_core(): lax.all_to_all(value, 'ep', 0, 0, axis_index_groups=rings, tiled=True)]
    ppermute x25 -> x24, starting transfers between devices: 45.1 us -> 41.5 us  [turned(): lax.ppermute(value, axis, [(i, (i + by) % peers) for i in range(peers)])]
  transfers between devices with their start and end apart: 33 -> 32, of which waited for: 15 -> 15; matrix products, arithmetic and copies ran while one was open for 9% -> 8% of each run, Pallas kernels for 13% -> 13%
where the time goes in v2:
time: 273 us; the launch traced here: 272 us
  waiting for transfers between devices  106 us (39%)
  starting transfers between devices  97.4 us (36%)
  Pallas kernels  34.5 us (13%)
  other arithmetic  16 us (6%)
  matrix products  10.8 us (4%)
  local copies, waits for them, and re-layouts  6.56 us (2%)
    ppermute x24, waiting for transfers between devices, turned(): lax.ppermute(value, axis, [(i, (i + by) % peers) for i in range(peers)])  77.7 us
    all_to_all x4, starting transfers between devices, same_core(): lax.all_to_all(value, 'ep', 0, 0, axis_index_groups=rings, tiled=True)  54.2 us
    ppermute x24, starting transfers between devices, turned(): lax.ppermute(value, axis, [(i, (i + by) % peers) for i in range(peers)])  41.5 us
    pallas_call x2, Pallas kernels, expert_rows(): pl.pallas_call(expert_kernel(in_counts, out_counts, holders, local_expert...  29.8 us
    all_to_all x4, waiting for transfers between devices, same_core(): lax.all_to_all(value, 'ep', 0, 0, axis_index_groups=rings, tiled=True)  27.5 us
  transfers between devices with their start and end apart: 32, of which 15 were waited for; matrix products, arithmetic and copies ran while one was open for 8% of the time, Pallas kernels for 13%

profile of v2, /device:TPU:40, one launch (start us, length us, event | category | flops | bytes accessed | tf_op | source)
XLA Modules:
  0.0 272.3 jit_solution(161866157455501593)
XLA Ops:
  2.5 1.2 convert_reduce_fusion.1
  3.7 1.3 fusion.12
  5.0 1.5 fusion.14
  6.6 1.2 fusion.1
  7.8 24.1 %all-to-all-start.2 = ((bf16[16,8,2176]{2,1,0:T(8,128)(2,1)}), bf16[16,8,2176]{2,1,0:T(8,128)(2,1)S(1)}, u32[]{:S(2)}, u32[]{:S(2)}) async-start(bf16[16,8,2176]{2,1,0:T(8,128)(2,1)} %fusion.1), calls=%async_computation.2 | async-start | bytes 1114112 | tf_op jit(solution)/shard_map/all_to_all | solution.py:93
  31.9 1.2 fusion
  34.2 27.5 %all-to-all-done.2 = bf16[16,8,2176]{2,1,0:T(8,128)(2,1)S(1)} async-done(((bf16[16,8,2176]{2,1,0:T(8,128)(2,1)}), bf16[16,8,2176]{2,1,0:T(8,128)(2,1)S(1)}, u32[]{:S(2)}, u32[]{:S(2)}) %all-to-all-start.2) | async-done | bytes 557088 | tf_op jit(solution)/shard_map/all_to_all | solution.py:93
  61.7 7.1 %all-to-all-start = ((bf16[16,8,2176]{2,1,0:T(8,128)(2,1)}), bf16[16,8,2176]{2,1,0:T(8,128)(2,1)S(1)}, u32[]{:S(2)}, u32[]{:S(2)}) async-start(bf16[16,8,2176]{2,1,0:T(8,128)(2,1)} %fusion), calls=%async_computation | async-start | bytes 1114112 | tf_op jit(solution)/shard_map/all_to_all | solution.py:93
  69.8 1.7 collective-permute-start.19
  71.5 1.7 collective-permute-start.20
  73.2 2.0 collective-permute-start.21
  75.8 1.2 fusion.11
  78.0 1.8 collective-permute-start.2
  79.8 5.9 %collective-permute-done.19.refs_1_ = bf16[128,2176]{1,0:T(8,128)(2,1)S(1)} collective-permute-done((bf16[128,2176]{1,0:T(8,128)(2,1)S(1)}, bf16[128,2176]{1,0:T(8,128)(2,1)S(1)}, u32[]{:S(2)}, u32[]{:S(2)}) %collective-permute-start.19) | collective-permute-done | bytes 557088 | tf_op jit(solution)/shard_map/ppermute | solution.py:27
  85.7 1.4 collective-permute-start
  87.0 10.8 %collective-permute-done.20.refs_2_ = bf16[128,2176]{1,0:T(8,128)(2,1)S(1)} collective-permute-done((bf16[128,2176]{1,0:T(8,128)(2,1)S(1)}, bf16[128,2176]{1,0:T(8,128)(2,1)S(1)}, u32[]{:S(2)}, u32[]{:S(2)}) %collective-permute-start.20) | collective-permute-done | bytes 557088 | tf_op jit(solution)/shard_map/ppermute | solution.py:27
  98.6 1.5 collective-permute-done.21.refs_3_
  100.1 14.9 %experts.3 = (bf16[128,2048]{1,0:T(8,128)(2,1)}, bf16[64,2048]{1,0:T(8,128)(2,1)}, bf16[64,2048]{1,0:T(8,128)(2,1)}, bf16[64,2048]{1,0:T(8,128)(2,1)}, bf16[64,2...) custom-call(bf16[128,2176]{1,0:T(8,128)(2,1)} %bitcast.89, bf16[128,2176]{1,0:T(8,128)(2,1)} %copy-done.13, ...), custom_call_target="tpu_custom_call" | custom-call | flops 6442450944 | bytes 16908288 | tf_op jit(solution)/shard_map/experts/pallas_call | solution.py:229
  115.1 2.6 collective-permute-start.26
  117.8 8.0 %collective-permute-start.7 = (bf16[128,2176]{1,0:T(8,128)(2,1)S(1)}, bf16[128,2176]{1,0:T(8,128)(2,1)}, u32[]{:S(2)}, u32[]{:S(2)}) collective-permute-start(bf16[128,2176]{1,0:T(8,128)(2,1)S(1)} %bitcast.82), channel_id=1, source_target_pairs={{0,1},{1,2},{2,3},{3,0},{4,5},{5,6},{6,7},{7,4},{8,9},{9,10},{10,1... | collective-permute-start | bytes 1671176 | tf_op jit(solution)/shard_map/ppermute | solution.py:27
  125.8 5.6 %collective-permute-done.26 = bf16[64,2048]{1,0:T(8,128)(2,1)S(1)} collective-permute-done((bf16[64,2048]{1,0:T(8,128)(2,1)}, bf16[64,2048]{1,0:T(8,128)(2,1)S(1)}, u32[]{:S(2)}, u32[]{:S(2)}) %collective-permute-start.26) | collective-permute-done | bytes 262176 | tf_op jit(solution)/shard_map/ppermute | solution.py:27
  131.4 1.0 collective-permute-start.22
  133.4 2.3 collective-permute-start.8
  135.9 2.3 collective-permute-start.24
  138.2 12.0 %collective-permute-done.22 = bf16[64,2048]{1,0:T(8,128)(2,1)S(1)} collective-permute-done((bf16[64,2048]{1,0:T(8,128)(2,1)}, bf16[64,2048]{1,0:T(8,128)(2,1)S(1)}, u32[]{:S(2)}, u32[]{:S(2)}) %collective-permute-start.22) | collective-permute-done | bytes 262176 | tf_op jit(solution)/shard_map/ppermute | solution.py:27
  151.2 11.1 %collective-permute-done.24.refs_1_ = bf16[64,2048]{1,0:T(8,128)(2,1)S(1)} collective-permute-done((bf16[64,2048]{1,0:T(8,128)(2,1)}, bf16[64,2048]{1,0:T(8,128)(2,1)S(1)}, u32[]{:S(2)}, u32[]{:S(2)}) %collective-permute-start.24) | collective-permute-done | bytes 262176 | tf_op jit(solution)/shard_map/ppermute | solution.py:27
  162.3 3.1 %collective-permute-start.27 = (bf16[64,2048]{1,0:T(8,128)(2,1)S(1)}, bf16[64,2048]{1,0:T(8,128)(2,1)S(1)}, u32[]{:S(2)}, u32[]{:S(2)}) collective-permute-start(bf16[64,2048]{1,0:T(8,128)(2,1)S(1)} %add_convert_fusion), channel_id=1, source_target_pairs={{0,3},{1,0},{2,1},{3,2},{4,7},{5,4},{6,5},{7,6},{8,11},{9,8},{10,9... | collective-permute-start | bytes 786440 | tf_op jit(solution)/shard_map/ppermute | solution.py:27
  166.2 2.8 %pad_maximum_fusion = bf16[4,128,2048]{2,1,0:T(8,128)(2,1)} fusion(bf16[1,128,2048]{2,1,0:T(8,128)(2,1)} %bitcast.11, bf16[1,128,2048]{2,1,0:T(8,128)(2,1)S(1)} %bitcast.90, bf16[1,128,2048]{2,1,0:T(8,128)(2,1)} %bitcast.9, bf16[1,128,2048]{2,1,0:T(8,128)(2,1)S(1)} %fusion.94), kind=kLoop, calls=%fused_computation.8 | loop fusion | flops 3145728 | bytes 4194304 | tf_op jit(solution)/shard_map/stack | solution.py:343
  169.3 3.7 %collective-permute-done.23.refs_0_ = bf16[64,2048]{1,0:T(8,128)(2,1)S(1)} collective-permute-done((bf16[64,2048]{1,0:T(8,128)(2,1)S(1)}, bf16[64,2048]{1,0:T(8,128)(2,1)S(1)}, u32[]{:S(2)}, u32[]{:S(2)}) %collective-permute-start.23) | collective-permute-done | bytes 262176 | tf_op jit(solution)/shard_map/ppermute | solution.py:27
  173.7 2.3 add_halves.3
  176.1 11.4 %all-to-all-start.3 = ((bf16[16,8,2048]{2,1,0:T(8,128)(2,1)}), bf16[16,8,2048]{2,1,0:T(8,128)(2,1)S(1)}, u32[]{:S(2)}, u32[]{:S(2)}) async-start(bf16[16,8,2048]{2,1,0:T(8,128)(2,1)} %bitcast.78), calls=%async_computation.3 | async-start | bytes 1048576 | tf_op jit(solution)/shard_map/all_to_all | solution.py:93
  187.5 14.9 %experts.2 = (bf16[128,2048]{1,0:T(8,128)(2,1)}, bf16[64,2048]{1,0:T(8,128)(2,1)}, bf16[64,2048]{1,0:T(8,128)(2,1)}, bf16[64,2048]{1,0:T(8,128)(2,1)}, bf16[64,2...) custom-call(bf16[128,2176]{1,0:T(8,128)(2,1)} %bitcast.85, ...), custom_call_target="tpu_custom_call" | custom-call | flops 6442450944 | bytes 16908288 | tf_op jit(solution)/shard_map/experts/pallas_call | solution.py:229
  202.6 2.6 convolution_convert_fusion.3
  205.3 2.1 collective-permute-start.13
  207.4 1.3 collective-permute-start.15
  209.5 3.8 %collective-permute-start.18 = (bf16[64,2048]{1,0:T(8,128)(2,1)S(1)}, bf16[64,2048]{1,0:T(8,128)(2,1)}, u32[]{:S(2)}, u32[]{:S(2)}) collective-permute-start(bf16[64,2048]{1,0:T(8,128)(2,1)S(1)} %add_convert_fusion.2), channel_id=1, source_target_pairs={{0,3},{1,0},{2,1},{3,2},{4,7},{5,4},{6,5},{7,6},{8,11},{9,8},{10,9... | collective-permute-start | bytes 786440 | tf_op jit(solution)/shard_map/ppermute | solution.py:27
  214.6 1.3 collective-permute-start.3
  217.1 4.3 %collective-permute-done.14.refs_0_ = bf16[64,2048]{1,0:T(8,128)(2,1)S(1)} collective-permute-done((bf16[64,2048]{1,0:T(8,128)(2,1)S(1)}, bf16[64,2048]{1,0:T(8,128)(2,1)S(1)}, u32[]{:S(2)}, u32[]{:S(2)}) %collective-permute-start.14) | collective-permute-done | bytes 262176 | tf_op jit(solution)/shard_map/ppermute | solution.py:27
  222.2 2.3 add_halves.2
  224.5 11.5 %all-to-all-start.1 = ((bf16[16,8,2048]{2,1,0:T(8,128)(2,1)}), bf16[16,8,2048]{2,1,0:T(8,128)(2,1)S(1)}, u32[]{:S(2)}, u32[]{:S(2)}) async-start(bf16[16,8,2048]{2,1,0:T(8,128)(2,1)} %bitcast.79), calls=%async_computation.1 | async-start | bytes 1048576 | tf_op jit(solution)/shard_map/all_to_all | solution.py:93
  236.1 4.2 %convolution_convert_fusion.2 = bf16[512,2048]{1,0:T(8,128)(2,1)} fusion(bf16[256,2048]{1,0:T(8,128)(2,1)S(1)} %copy-done, f32[256]{0:T(256)S(1)} %copy-done.16, f32[527,256]{1,0:T(8,128)S(1)} %maximum_convert_fusion, s32[256]{0:T(256)S(1)} %fusion.82, s32[512]{0:T(512)S(1)} %add_add_fusion, pred[256]{0:T(512)(128)(4,1)S(1)} %get-tuple-element.53, ...), kind=kOutput, calls=%fused_computation.5 | convolution fusion | flops 609878016 | bytes 11677184 | tf_op jit(solution)/shard_map/dot_general | solution.py:355
  240.3 2.3 dynamic-slice_bitcast_fusion.2
  242.6 2.6 collective-permute-start.4
  245.3 1.5 collective-permute-start.6
  246.7 18.4 %collective-permute-done.4 = bf16[128,2048]{1,0:T(8,128)(2,1)} collective-permute-done((bf16[128,2048]{1,0:T(8,128)(2,1)}, bf16[128,2048]{1,0:T(8,128)(2,1)}, u32[]{:S(2)}, u32[]{:S(2)}) %collective-permute-start.4) | collective-permute-done | bytes 524320 | tf_op jit(solution)/shard_map/ppermute | solution.py:27
  265.1 3.2 %collective-permute-done.5 = bf16[128,2048]{1,0:T(8,128)(2,1)} collective-permute-done((bf16[128,2048]{1,0:T(8,128)(2,1)S(1)}, bf16[128,2048]{1,0:T(8,128)(2,1)}, u32[]{:S(2)}, u32[]{:S(2)}) %collective-permute-start.5) | collective-permute-done | bytes 524320 | tf_op jit(solution)/shard_map/ppermute | solution.py:27
  268.3 2.6 fusion.17
  271.2 1.1 fusion.2
  (112 shorter events, 14.9 us)
Async XLA Ops:
  0.6 235.4 %copy-start = (bf16[256,2048]{1,0:T(8,128)(2,1)S(1)}, bf16[256,2048]{1,0:T(8,128)(2,1)}, u32[]{:S(2)}) copy-start(bf16[256,2048]{1,0:T(8,128)(2,1)} %param.18) | copy-start | bytes 3145732
  5.0 28.7 %copy-start.1 = (bf16[128,2048]{1,0:T(8,128)(2,1)S(1)}, bf16[128,2048]{1,0:T(8,128)(2,1)}, u32[]{:S(2)}) copy-start(bf16[128,2048]{1,0:T(8,128)(2,1)} %param.13) | copy-start | bytes 1572868
  7.8 61.6 %copy-start.12 = (f32[2048]{0:T(1024)S(1)}, f32[2048]{0:T(1024)}, u32[]{:S(2)}) copy-start(f32[2048]{0:T(1024)} %param.14) | copy-start | bytes 24580
  7.8 53.8 %all-to-all-start.2 = ((bf16[16,8,2176]{2,1,0:T(8,128)(2,1)}), bf16[16,8,2176]{2,1,0:T(8,128)(2,1)S(1)}, u32[]{:S(2)}, u32[]{:S(2)}) async-start(bf16[16,8,2176]{2,1,0:T(8,128)(2,1)} %fusion.1), calls=%async_computation.2 | async-start | bytes 1114112 | tf_op jit(solution)/shard_map/all_to_all | solution.py:93
  33.1 40.1 %collective-permute-start.10 = (bf16[2,2048,256]{2,1,0:T(8,128)(2,1)}, bf16[2,2048,256]{2,1,0:T(8,128)(2,1)}, u32[]{:S(2)}, u32[]{:S(2)}) collective-permute-start(bf16[2,2048,256]{2,1,0:T(8,128)(2,1)} %refs_4_.1), channel_id=1, source_target_pairs={{0,4},{4,0},{8,12},{12,8},{16,20},{20,16},{24,28},{28,24},{32,36},... | collective-permute-start | bytes 6291464 | tf_op jit(solution)/shard_map/ppermute | solution.py:324
  33.1 43.9 %collective-permute-start.11 = (bf16[2,2048,256]{2,1,0:T(8,128)(2,1)}, bf16[2,2048,256]{2,1,0:T(8,128)(2,1)}, u32[]{:S(2)}, u32[]{:S(2)}) collective-permute-start(bf16[2,2048,256]{2,1,0:T(8,128)(2,1)} %refs_5_.1), channel_id=1, source_target_pairs={{0,4},{4,0},{8,12},{12,8},{16,20},{20,16},{24,28},{28,24},{32,36},... | collective-permute-start | bytes 6291464 | tf_op jit(solution)/shard_map/ppermute | solution.py:324
  33.6 44.4 %collective-permute-start.12 = (bf16[2,256,2048]{2,1,0:T(8,128)(2,1)}, bf16[2,256,2048]{2,1,0:T(8,128)(2,1)}, u32[]{:S(2)}, u32[]{:S(2)}) collective-permute-start(bf16[2,256,2048]{2,1,0:T(8,128)(2,1)} %refs_6_.1), channel_id=1, source_target_pairs={{0,4},{4,0},{8,12},{12,8},{16,20},{20,16},{24,28},{28,24},{32,36},... | collective-permute-start | bytes 6291464 | tf_op jit(solution)/shard_map/ppermute | solution.py:324
  61.7 38.5 %copy-start.3 = (bf16[16,8,2176]{2,1,0:T(8,128)(2,1)}, bf16[16,8,2176]{2,1,0:T(8,128)(2,1)S(1)}, u32[]{:S(2)}) copy-start(bf16[16,8,2176]{2,1,0:T(8,128)(2,1)S(1)} %all-to-all-done.2) | copy-start | bytes 1671172
  61.7 56.1 %all-to-all-start = ((bf16[16,8,2176]{2,1,0:T(8,128)(2,1)}), bf16[16,8,2176]{2,1,0:T(8,128)(2,1)S(1)}, u32[]{:S(2)}, u32[]{:S(2)}) async-start(bf16[16,8,2176]{2,1,0:T(8,128)(2,1)} %fusion), calls=%async_computation | async-start | bytes 1114112 | tf_op jit(solution)/shard_map/all_to_all | solution.py:93
  69.8 15.9 %collective-permute-start.19 = (bf16[128,2176]{1,0:T(8,128)(2,1)S(1)}, bf16[128,2176]{1,0:T(8,128)(2,1)S(1)}, u32[]{:S(2)}, u32[]{:S(2)}) collective-permute-start(bf16[128,2176]{1,0:T(8,128)(2,1)S(1)} %bitcast.86), channel_id=1, source_target_pairs={{0,1},{1,2},{2,3},{3,0},{4,5},{5,6},{6,7},{7,4},{8,9},{9,10},{10,1... | collective-permute-start | bytes 1671176 | tf_op jit(solution)/shard_map/ppermute | solution.py:27
  71.5 26.3 %collective-permute-start.20 = (bf16[128,2176]{1,0:T(8,128)(2,1)S(1)}, bf16[128,2176]{1,0:T(8,128)(2,1)S(1)}, u32[]{:S(2)}, u32[]{:S(2)}) collective-permute-start(bf16[128,2176]{1,0:T(8,128)(2,1)S(1)} %bitcast.87), channel_id=1, source_target_pairs={{0,3},{1,0},{2,1},{3,2},{4,7},{5,4},{6,5},{7,6},{8,11},{9,8},{10,9... | collective-permute-start | bytes 1671176 | tf_op jit(solution)/shard_map/ppermute | solution.py:27
  73.2 26.9 %collective-permute-start.21 = (bf16[128,2176]{1,0:T(8,128)(2,1)S(1)}, bf16[128,2176]{1,0:T(8,128)(2,1)}, u32[]{:S(2)}, u32[]{:S(2)}) collective-permute-start(bf16[128,2176]{1,0:T(8,128)(2,1)S(1)} %bitcast.88), channel_id=1, source_target_pairs={{0,2},{1,3},{2,0},{3,1},{4,6},{5,7},{6,4},{7,5},{8,10},{9,11},{10,... | collective-permute-start | bytes 1671176 | tf_op jit(solution)/shard_map/ppermute | solution.py:27
  77.0 56.4 %collective-permute-start.1 = (bf16[128,2048]{1,0:T(8,128)(2,1)}, bf16[128,2048]{1,0:T(8,128)(2,1)S(1)}, u32[]{:S(2)}, u32[]{:S(2)}) collective-permute-start(bf16[128,2048]{1,0:T(8,128)(2,1)} %fusion.11), channel_id=1, source_target_pairs={{0,3},{1,0},{2,1},{3,2},{4,7},{5,4},{6,5},{7,6},{8,11},{9,8},{10,9... | collective-permute-start | bytes 1572872 | tf_op jit(solution)/shard_map/ppermute | solution.py:27
  78.0 57.8 %collective-permute-start.2 = (bf16[128,2048]{1,0:T(8,128)(2,1)}, bf16[128,2048]{1,0:T(8,128)(2,1)}, u32[]{:S(2)}, u32[]{:S(2)}) collective-permute-start(bf16[128,2048]{1,0:T(8,128)(2,1)} %fusion.11), channel_id=1, source_target_pairs={{0,2},{1,3},{2,0},{3,1},{4,6},{5,7},{6,4},{7,5},{8,10},{9,11},{10,... | collective-permute-start | bytes 1572872 | tf_op jit(solution)/shard_map/ppermute | solution.py:27
  85.7 12.2 %copy-start.13 = (bf16[128,2176]{1,0:T(8,128)(2,1)}, bf16[128,2176]{1,0:T(8,128)(2,1)S(1)}, u32[]{:S(2)}) copy-start(bf16[128,2176]{1,0:T(8,128)(2,1)S(1)} %collective-permute-done.19.refs_1_) | copy-start | bytes 1671172
  85.7 50.3 %collective-permute-start = (bf16[128,2048]{1,0:T(8,128)(2,1)}, bf16[128,2048]{1,0:T(8,128)(2,1)}, u32[]{:S(2)}, u32[]{:S(2)}) collective-permute-start(bf16[128,2048]{1,0:T(8,128)(2,1)} %fusion.11), channel_id=1, source_target_pairs={{0,1},{1,2},{2,3},{3,0},{4,5},{5,6},{6,7},{7,4},{8,9},{9,10},{10,1... | collective-permute-start | bytes 1572872 | tf_op jit(solution)/shard_map/ppermute | solution.py:27
  115.1 16.3 %collective-permute-start.26 = (bf16[64,2048]{1,0:T(8,128)(2,1)}, bf16[64,2048]{1,0:T(8,128)(2,1)S(1)}, u32[]{:S(2)}, u32[]{:S(2)}) collective-permute-start(bf16[64,2048]{1,0:T(8,128)(2,1)} %get-tuple-element.39), channel_id=1, source_target_pairs={{0,3},{1,0},{2,1},{3,2},{4,7},{5,4},{6,5},{7,6},{8,11},{9,8},{10,9... | collective-permute-start | bytes 786440 | tf_op jit(solution)/shard_map/ppermute | solution.py:27
  117.8 51.2 %copy-start.2 = (bf16[16,8,2176]{2,1,0:T(8,128)(2,1)}, bf16[16,8,2176]{2,1,0:T(8,128)(2,1)S(1)}, u32[]{:S(2)}) copy-start(bf16[16,8,2176]{2,1,0:T(8,128)(2,1)S(1)} %all-to-all-done) | copy-start | bytes 1671172
  117.8 69.7 %collective-permute-start.7 = (bf16[128,2176]{1,0:T(8,128)(2,1)S(1)}, bf16[128,2176]{1,0:T(8,128)(2,1)}, u32[]{:S(2)}, u32[]{:S(2)}) collective-permute-start(bf16[128,2176]{1,0:T(8,128)(2,1)S(1)} %bitcast.82), channel_id=1, source_target_pairs={{0,1},{1,2},{2,3},{3,0},{4,5},{5,6},{6,7},{7,4},{8,9},{9,10},{10,1... | collective-permute-start | bytes 1671176 | tf_op jit(solution)/shard_map/ppermute | solution.py:27
  131.4 18.9 %collective-permute-start.22 = (bf16[64,2048]{1,0:T(8,128)(2,1)}, bf16[64,2048]{1,0:T(8,128)(2,1)S(1)}, u32[]{:S(2)}, u32[]{:S(2)}) collective-permute-start(bf16[64,2048]{1,0:T(8,128)(2,1)} %get-tuple-element.35), channel_id=1, source_target_pairs={{0,1},{1,2},{2,3},{3,0},{4,5},{5,6},{6,7},{7,4},{8,9},{9,10},{10,1... | collective-permute-start | bytes 786440 | tf_op jit(solution)/shard_map/ppermute | solution.py:27
  133.4 54.1 %collective-permute-start.8 = (bf16[128,2176]{1,0:T(8,128)(2,1)S(1)}, bf16[128,2176]{1,0:T(8,128)(2,1)}, u32[]{:S(2)}, u32[]{:S(2)}) collective-permute-start(bf16[128,2176]{1,0:T(8,128)(2,1)S(1)} %bitcast.83), channel_id=1, source_target_pairs={{0,3},{1,0},{2,1},{3,2},{4,7},{5,4},{6,5},{7,6},{8,11},{9,8},{10,9... | collective-permute-start | bytes 1671176 | tf_op jit(solution)/shard_map/ppermute | solution.py:27
  135.7 51.7 %collective-permute-start.9 = (bf16[128,2176]{1,0:T(8,128)(2,1)S(1)}, bf16[128,2176]{1,0:T(8,128)(2,1)}, u32[]{:S(2)}, u32[]{:S(2)}) collective-permute-start(bf16[128,2176]{1,0:T(8,128)(2,1)S(1)} %bitcast.84), channel_id=1, source_target_pairs={{0,2},{1,3},{2,0},{3,1},{4,6},{5,7},{6,4},{7,5},{8,10},{9,11},{10,... | collective-permute-start | bytes 1671176 | tf_op jit(solution)/shard_map/ppermute | solution.py:27
  135.9 26.4 %collective-permute-start.24 = (bf16[64,2048]{1,0:T(8,128)(2,1)}, bf16[64,2048]{1,0:T(8,128)(2,1)S(1)}, u32[]{:S(2)}, u32[]{:S(2)}) collective-permute-start(bf16[64,2048]{1,0:T(8,128)(2,1)} %get-tuple-element.36), channel_id=1, source_target_pairs={{0,3},{1,0},{2,1},{3,2},{4,7},{5,4},{6,5},{7,6},{8,11},{9,8},{10,9... | collective-permute-start | bytes 786440 | tf_op jit(solution)/shard_map/ppermute | solution.py:27
  150.2 15.2 %collective-permute-start.25 = (bf16[64,2048]{1,0:T(8,128)(2,1)}, bf16[64,2048]{1,0:T(8,128)(2,1)S(1)}, u32[]{:S(2)}, u32[]{:S(2)}) collective-permute-start(bf16[64,2048]{1,0:T(8,128)(2,1)} %get-tuple-element.37), channel_id=1, source_target_pairs={{0,1},{1,2},{2,3},{3,0},{4,5},{5,6},{6,7},{7,4},{8,9},{9,10},{10,1... | collective-permute-start | bytes 786440 | tf_op jit(solution)/shard_map/ppermute | solution.py:27
  162.3 6.6 %copy-start.8 = (bf16[64,2048]{1,0:T(8,128)(2,1)}, bf16[64,2048]{1,0:T(8,128)(2,1)S(1)}, u32[]{:S(2)}) copy-start(bf16[64,2048]{1,0:T(8,128)(2,1)S(1)} %collective-permute-done.24.refs_1_) | copy-start | bytes 786436
  162.3 7.0 %collective-permute-start.27 = (bf16[64,2048]{1,0:T(8,128)(2,1)S(1)}, bf16[64,2048]{1,0:T(8,128)(2,1)S(1)}, u32[]{:S(2)}, u32[]{:S(2)}) collective-permute-start(bf16[64,2048]{1,0:T(8,128)(2,1)S(1)} %add_convert_fusion), channel_id=1, source_target_pairs={{0,3},{1,0},{2,1},{3,2},{4,7},{5,4},{6,5},{7,6},{8,11},{9,8},{10,9... | collective-permute-start | bytes 786440 | tf_op jit(solution)/shard_map/ppermute | solution.py:27
  165.5 7.6 %collective-permute-start.23 = (bf16[64,2048]{1,0:T(8,128)(2,1)S(1)}, bf16[64,2048]{1,0:T(8,128)(2,1)S(1)}, u32[]{:S(2)}, u32[]{:S(2)}) collective-permute-start(bf16[64,2048]{1,0:T(8,128)(2,1)S(1)} %add_convert_fusion.1), channel_id=1, source_target_pairs={{0,1},{1,2},{2,3},{3,0},{4,5},{5,6},{6,7},{7,4},{8,9},{9,10},{10,1... | collective-permute-start | bytes 786440 | tf_op jit(solution)/shard_map/ppermute | solution.py:27
  169.3 4.4 %copy-start.10 = (bf16[64,2048]{1,0:T(8,128)(2,1)}, bf16[64,2048]{1,0:T(8,128)(2,1)S(1)}, u32[]{:S(2)}) copy-start(bf16[64,2048]{1,0:T(8,128)(2,1)S(1)} %collective-permute-done.27.refs_3_) | copy-start | bytes 786436
  176.1 48.5 %all-to-all-start.3 = ((bf16[16,8,2048]{2,1,0:T(8,128)(2,1)}), bf16[16,8,2048]{2,1,0:T(8,128)(2,1)S(1)}, u32[]{:S(2)}, u32[]{:S(2)}) async-start(bf16[16,8,2048]{2,1,0:T(8,128)(2,1)} %bitcast.78), calls=%async_computation.3 | async-start | bytes 1048576 | tf_op jit(solution)/shard_map/all_to_all | solution.py:93
  202.4 7.0 %collective-permute-start.17 = (bf16[64,2048]{1,0:T(8,128)(2,1)}, bf16[64,2048]{1,0:T(8,128)(2,1)S(1)}, u32[]{:S(2)}, u32[]{:S(2)}) collective-permute-start(bf16[64,2048]{1,0:T(8,128)(2,1)} %get-tuple-element.32), channel_id=1, source_target_pairs={{0,3},{1,0},{2,1},{3,2},{4,7},{5,4},{6,5},{7,6},{8,11},{9,8},{10,9... | collective-permute-start | bytes 786440 | tf_op jit(solution)/shard_map/ppermute | solution.py:27
  202.6 2.7 copy-start.15
  202.6 6.8 %copy-start.5 = (bf16[64,2048]{1,0:T(8,128)(2,1)S(1)}, bf16[64,2048]{1,0:T(8,128)(2,1)}, u32[]{:S(2)}) copy-start(bf16[64,2048]{1,0:T(8,128)(2,1)} %get-tuple-element.31) | copy-start | bytes 786436
  202.6 11.1 %copy-start.4 = (bf16[64,2048]{1,0:T(8,128)(2,1)S(1)}, bf16[64,2048]{1,0:T(8,128)(2,1)}, u32[]{:S(2)}) copy-start(bf16[64,2048]{1,0:T(8,128)(2,1)} %get-tuple-element.27) | copy-start | bytes 786436
  205.3 8.4 %collective-permute-start.13 = (bf16[64,2048]{1,0:T(8,128)(2,1)S(1)}, bf16[64,2048]{1,0:T(8,128)(2,1)S(1)}, u32[]{:S(2)}, u32[]{:S(2)}) collective-permute-start(bf16[64,2048]{1,0:T(8,128)(2,1)S(1)} %copy-done.15), channel_id=1, source_target_pairs={{0,1},{1,2},{2,3},{3,0},{4,5},{5,6},{6,7},{7,4},{8,9},{9,10},{10,1... | collective-permute-start | bytes 786440 | tf_op jit(solution)/shard_map/ppermute | solution.py:27
  207.4 9.4 %collective-permute-start.15 = (bf16[64,2048]{1,0:T(8,128)(2,1)}, bf16[64,2048]{1,0:T(8,128)(2,1)S(1)}, u32[]{:S(2)}, u32[]{:S(2)}) collective-permute-start(bf16[64,2048]{1,0:T(8,128)(2,1)} %get-tuple-element.29), channel_id=1, source_target_pairs={{0,3},{1,0},{2,1},{3,2},{4,7},{5,4},{6,5},{7,6},{8,11},{9,8},{10,9... | collective-permute-start | bytes 786440 | tf_op jit(solution)/shard_map/ppermute | solution.py:27
  208.6 8.2 %collective-permute-start.16 = (bf16[64,2048]{1,0:T(8,128)(2,1)}, bf16[64,2048]{1,0:T(8,128)(2,1)}, u32[]{:S(2)}, u32[]{:S(2)}) collective-permute-start(bf16[64,2048]{1,0:T(8,128)(2,1)} %get-tuple-element.30), channel_id=1, source_target_pairs={{0,1},{1,2},{2,3},{3,0},{4,5},{5,6},{6,7},{7,4},{8,9},{9,10},{10,1... | collective-permute-start | bytes 786440 | tf_op jit(solution)/shard_map/ppermute | solution.py:27
  209.5 7.7 %collective-permute-start.18 = (bf16[64,2048]{1,0:T(8,128)(2,1)S(1)}, bf16[64,2048]{1,0:T(8,128)(2,1)}, u32[]{:S(2)}, u32[]{:S(2)}) collective-permute-start(bf16[64,2048]{1,0:T(8,128)(2,1)S(1)} %add_convert_fusion.2), channel_id=1, source_target_pairs={{0,3},{1,0},{2,1},{3,2},{4,7},{5,4},{6,5},{7,6},{8,11},{9,8},{10,9... | collective-permute-start | bytes 786440 | tf_op jit(solution)/shard_map/ppermute | solution.py:27
  213.8 7.7 %collective-permute-start.14 = (bf16[64,2048]{1,0:T(8,128)(2,1)S(1)}, bf16[64,2048]{1,0:T(8,128)(2,1)S(1)}, u32[]{:S(2)}, u32[]{:S(2)}) collective-permute-start(bf16[64,2048]{1,0:T(8,128)(2,1)S(1)} %add_convert_fusion.3), channel_id=1, source_target_pairs={{0,1},{1,2},{2,3},{3,0},{4,5},{5,6},{6,7},{7,4},{8,9},{9,10},{10,1... | collective-permute-start | bytes 786440 | tf_op jit(solution)/shard_map/ppermute | solution.py:27
  214.5 21.5 %copy-start.16 = (f32[256]{0:T(256)S(1)}, f32[256]{0:T(256)}, u32[]{:S(2)}) copy-start(f32[256]{0:T(256)} %param.17) | copy-start | bytes 3076
  214.6 21.5 %copy-start.17 = (pred[256]{0:T(512)(128)(4,1)S(1)}, pred[256]{0:T(512)(128)(4,1)}, u32[]{:S(2)}) copy-start(pred[256]{0:T(512)(128)(4,1)} %get-tuple-element.64) | copy-start | bytes 772
  214.6 21.5 %copy-start.18 = (pred[256]{0:T(512)(128)(4,1)S(1)}, pred[256]{0:T(512)(128)(4,1)}, u32[]{:S(2)}) copy-start(pred[256]{0:T(512)(128)(4,1)} %get-tuple-element.65) | copy-start | bytes 772
  214.6 21.5 %copy-start.19 = (pred[256]{0:T(512)(128)(4,1)S(1)}, pred[256]{0:T(512)(128)(4,1)}, u32[]{:S(2)}) copy-start(pred[256]{0:T(512)(128)(4,1)} %get-tuple-element.66) | copy-start | bytes 772
  214.6 2.1 collective-permute-start.3
  216.8 4.7 %copy-start.6 = (bf16[64,2048]{1,0:T(8,128)(2,1)}, bf16[64,2048]{1,0:T(8,128)(2,1)S(1)}, u32[]{:S(2)}) copy-start(bf16[64,2048]{1,0:T(8,128)(2,1)S(1)} %collective-permute-done.15.refs_1_) | copy-start | bytes 786436
  224.5 46.7 %all-to-all-start.1 = ((bf16[16,8,2048]{2,1,0:T(8,128)(2,1)}), bf16[16,8,2048]{2,1,0:T(8,128)(2,1)S(1)}, u32[]{:S(2)}, u32[]{:S(2)}) async-start(bf16[16,8,2048]{2,1,0:T(8,128)(2,1)} %bitcast.79), calls=%async_computation.1 | async-start | bytes 1048576 | tf_op jit(solution)/shard_map/all_to_all | solution.py:93
  242.6 22.5 %collective-permute-start.4 = (bf16[128,2048]{1,0:T(8,128)(2,1)}, bf16[128,2048]{1,0:T(8,128)(2,1)}, u32[]{:S(2)}, u32[]{:S(2)}) collective-permute-start(bf16[128,2048]{1,0:T(8,128)(2,1)} %get-tuple-element.42), channel_id=1, source_target_pairs={{0,3},{1,0},{2,1},{3,2},{4,7},{5,4},{6,5},{7,6},{8,11},{9,8},{10,9... | collective-permute-start | bytes 1572872 | tf_op jit(solution)/shard_map/ppermute | solution.py:27
  245.3 23.0 %collective-permute-start.5 = (bf16[128,2048]{1,0:T(8,128)(2,1)S(1)}, bf16[128,2048]{1,0:T(8,128)(2,1)}, u32[]{:S(2)}, u32[]{:S(2)}) collective-permute-start(bf16[128,2048]{1,0:T(8,128)(2,1)S(1)} %get-tuple-element.44), channel_id=1, source_target_pairs={{0,1},{1,2},{2,3},{3,0},{4,5},{5,6},{6,7},{7,4},{8,9},{9,10},{10,1... | collective-permute-start | bytes 1572872 | tf_op jit(solution)/shard_map/ppermute | solution.py:27
  245.3 23.0 %collective-permute-start.6 = (bf16[128,2048]{1,0:T(8,128)(2,1)S(1)}, bf16[128,2048]{1,0:T(8,128)(2,1)}, u32[]{:S(2)}, u32[]{:S(2)}) collective-permute-start(bf16[128,2048]{1,0:T(8,128)(2,1)S(1)} %get-tuple-element.43), channel_id=1, source_target_pairs={{0,2},{1,3},{2,0},{3,1},{4,6},{5,7},{6,4},{7,5},{8,10},{9,11},{10,... | collective-permute-start | bytes 1572872 | tf_op jit(solution)/shard_map/ppermute | solution.py:27
  (4 other events, 2.9 us)
